TPU v7x, 32 devices: a whole 2x2x4 slice. The times are simulated.
32 devices in a mesh: sp: 8 (over z, x), tp: 4 (over y, core).
Axes of the slice: x: 2, y: 2, z: 4, core: 2. Of those that a mesh axis runs over, the one named last changes fastest.
Arguments:
- cotangent: bfloat16 [1024, 2048], P('sp'), may hold values from -6 to 6
- stream: bfloat16 [1024, 2048], P('sp'), may hold values from -6 to 6
- routes: int32 [1024, 2], P('sp'), may hold values from 0 to 3, all different within a row; in each aligned block of 128 rows (0 to 127, 128 to 255, ...) at most 96 rows name the same one
- route_weights: float32 [1024, 2], P('sp'), may hold values from 0.25 to 1
- gate_weight: bfloat16 [8, 2048, 2048], P('sp', None, 'tp'), may hold values from -0.125 to 0.125
- up_weight: bfloat16 [8, 2048, 2048], P('sp', None, 'tp'), may hold values from -0.125 to 0.125
- down_weight: bfloat16 [8, 2048, 2048], P('sp', 'tp'), may hold values from -0.09375 to 0.09375
- outer_gate: bfloat16 [1024, 1024], P('sp', 'tp'), may hold values from -6 to 6
- inner_gate: bfloat16 [1024, 1024], P('sp', 'tp'), may hold values from -6 to 6
- conv_input: bfloat16 [1024, 1024], P('sp', 'tp'), may hold values from -6 to 6
- conv_taps: bfloat16 [3, 1024], P(None, 'tp'), may hold values from -1 to 1
- out_weight: bfloat16 [2048, 1024], P(None, 'tp'), may hold values from -0.1875 to 0.1875
Outputs:
- gate_grad: bfloat16 [8, 2048, 2048], P('sp', None, 'tp')
- up_grad: bfloat16 [8, 2048, 2048], P('sp', None, 'tp')
- down_grad: bfloat16 [8, 2048, 2048], P('sp', 'tp')
- out_grad: float32 [2048, 1024], P('sp', 'tp')
- outer_grad: bfloat16 [1024, 1024], P('sp', 'tp')
- inner_grad: bfloat16 [1024, 1024], P('sp', 'tp')
- input_grad: bfloat16 [1024, 1024], P('sp', 'tp')
Inputs may be any that keep to these rules, and one draw needn't show every extreme that they name: `routes`: each token names two different experts. Among the 128 tokens of one index of sp no expert is named by more than 96 tokens, a bound that some block of them reaches in every draw.
All inputs are finite; a program needn't handle non-finite values.
Results may differ from a plain program's by a relative error of at most 0.02.
Values may be sent and summed in bfloat16 or wider, within the bound.
A program may use at most 64 MiB of HBM per device.

v0:
```python
import functools

import jax
import jax.numpy as jnp
from jax import lax
from jax.experimental import pallas as pl
from jax.experimental.pallas import tpu as pltpu
from jax.sharding import PartitionSpec as P


def from_behind(block, axis, distance):
    devices = range(lax.axis_size(axis))
    route = [(i - distance, i) for i in devices if i - distance in devices]
    return lax.ppermute(block, axis, route)


def near_first(count):
    return sorted(range(count), key=lambda d: (min(d, count - d), d))


class Seat:
    def __init__(self, experts, pairs):
        self.sp = lax.axis_index("sp")
        self.tp = lax.axis_index("tp")
        self.half = lax.rem(self.sp, 2)
        self.expert = self.sp // 2
        self.core = lax.rem(self.tp, 2)
        self.row = self.tp // 2
        self.experts = experts
        self.pairs = pairs

    def ahead(self, distance):
        return lax.rem(self.expert + distance, self.experts)

    def behind(self, distance):
        return lax.rem(self.expert + self.experts - distance, self.experts)

    def other_expert(self, expert):
        return (expert * 2 + self.half, self.tp)

    def next_tokens(self, distance):
        groups = 2 * self.experts
        return (lax.rem(self.sp + groups + distance, groups), self.tp)

    def other_half(self):
        return (self.expert * 2 + 1 - self.half, self.tp)

    def row_ahead(self, distance):
        return lax.rem(self.row + distance, self.pairs)

    def row_behind(self, distance):
        return lax.rem(self.row + self.pairs - distance, self.pairs)

    def other_row(self, row):
        return (self.sp, row * 2 + self.core)

    def other_core(self):
        return (self.sp, self.row * 2 + 1 - self.core)


def remote(src, dst, sent, landed, device):
    return pltpu.make_async_remote_copy(
        src_ref=src,
        dst_ref=dst,
        send_sem=sent,
        recv_sem=landed,
        device_id=device,
        device_id_type=pl.DeviceIdType.MESH,
    )


def greet(peers):
    barrier = pltpu.get_barrier_semaphore()
    for peer in peers:
        pl.semaphore_signal(barrier, inc=1, device_id=peer, device_id_type=pl.DeviceIdType.MESH)
    return lambda: pl.semaphore_wait(barrier, len(peers))


def dispatch_kernel(experts, pairs, routes_hbm, weights_hbm, stream_hbm, given_hbm, inner_hbm, input_hbm,
                    rows_ref, cot_ref, select_ref, early_ref, send_ref, tail_ref,
                    routes_ref, weights_ref, block_ref, edge_ref,
                    zs, zr, xs, xr, ys, yr, ds, dr, cs, cr, own, hs, hr, ls):
    seat = Seat(experts, pairs)
    capacity, width = send_ref.shape[2:]
    tokens = routes_ref.shape[1]
    offs = near_first(experts)
    outs = (rows_ref, cot_ref)
    all_here = greet(
        [seat.next_tokens(1), seat.next_tokens(-1)] +
        [seat.other_expert(seat.ahead(d)) for d in range(1, experts)]
        + [seat.other_half(), seat.other_core()]
        + [seat.other_row(seat.row_ahead(d)) for d in range(1, pairs)]
    )
    started = []
    mine = pl.ds(pl.multiple_of(seat.tp * width, width), width)
    edge = pl.ds(tokens - tail_ref.shape[0], tail_ref.shape[0])
    loads = [
        pltpu.make_async_copy(src, dst, ls.at[n])
        for n, (src, dst) in enumerate((
            (routes_hbm, routes_ref),
            (weights_hbm, weights_ref),
            (stream_hbm.at[:, mine], block_ref.at[0]),
            (inner_hbm.at[edge, :], edge_ref.at[0]),
            (input_hbm.at[edge, :], edge_ref.at[1]),
            (given_hbm.at[:, mine], block_ref.at[1]),
        ))
    ]
    for load in loads:
        load.start()
    for load in loads:
        load.wait()
    tail_ref[...] = edge_ref[0].astype(jnp.float32) * edge_ref[1].astype(jnp.float32)
    number = lax.broadcasted_iota(jnp.int32, (experts, tokens), 0)
    named = [routes_ref[k:k + 1, :] == number for k in range(2)]
    member = jnp.where(named[0] | named[1], 1.0, 0.0)
    share = jnp.where(named[0], weights_ref[0:1, :], 0.0) + jnp.where(
        named[1], weights_ref[1:2, :], 0.0
    )
    sooner = lax.broadcasted_iota(jnp.int32, (tokens, tokens), 0) < lax.broadcasted_iota(
        jnp.int32, (tokens, tokens), 1
    )
    rank = jnp.dot(
        member.astype(jnp.bfloat16),
        jnp.where(sooner, 1.0, 0.0).astype(jnp.bfloat16),
        preferred_element_type=jnp.float32,
    )
    slot = lax.broadcasted_iota(jnp.int32, (capacity, tokens), 0).astype(jnp.float32)
    slot_weight = []
    for e in range(experts):
        chosen = jnp.where(slot == rank[e:e + 1], member[e:e + 1], 0.0)
        slot_weight.append(jnp.sum(chosen * share[e:e + 1], axis=1, keepdims=True))
        select_ref[e * capacity:(e + 1) * capacity, :] = chosen.astype(jnp.bfloat16)

    def fill(kind):
        block = block_ref[kind]
        for e in range(experts):
            picked = jnp.dot(
                select_ref[e * capacity:(e + 1) * capacity, :], block,
                preferred_element_type=jnp.float32,
            )
            if kind:
                picked = picked * slot_weight[e]
            send_ref[kind, e] = picked.astype(jnp.bfloat16)

    def place(kind, half, expert, tp):
        cols = pl.ds(pl.multiple_of(tp * width, width), width)
        return outs[kind].at[half, expert, :, cols]

    def push(src, dst, sent, landed, device):
        copy = remote(src, dst, sent, landed, device)
        copy.start()
        started.append(copy)

    def landed(spot, sem_s, sem_r):
        remote(spot, spot, sem_s, sem_r, seat.other_core()).wait_recv()

    items = [(kind, k) for kind in range(2) for k in range(experts)]
    local = []
    for kind in range(2):
        fill(kind)
        if kind == 0:
            all_here()
        spot = place(kind, seat.half, seat.expert, seat.tp)
        copy = pltpu.make_async_copy(send_ref.at[kind, seat.expert], spot, own.at[kind])
        copy.start()
        local.append(copy)
        for k in range(1, experts):
            target = seat.behind(offs[k])
            push(send_ref.at[kind, target], spot, zs.at[kind, k], zr.at[kind, k],
                 seat.other_expert(target))

    push(tail_ref, early_ref, hs.at[0], hr.at[0], seat.next_tokens(1))

    def first(kind, k):
        spot = place(kind, seat.half, seat.ahead(offs[k]), seat.tp)
        if k == 0:
            src = send_ref.at[kind, seat.expert]
        else:
            landed(spot, zs.at[kind, k], zr.at[kind, k])
            src = spot
        push(src, spot, xs.at[kind, k], xr.at[kind, k], seat.other_half())
        for d in range(1, pairs):
            push(src, spot, ys.at[kind, k, d], yr.at[kind, k, d],
                 seat.other_row(seat.row_behind(d)))
        push(src, spot, cs.at[kind, k, 0], cr.at[kind, k, 0], seat.other_core())

    def second(kind, k):
        expert = seat.ahead(offs[k])
        spot = place(kind, 1 - seat.half, expert, seat.tp)
        landed(spot, xs.at[kind, k], xr.at[kind, k])
        if k % 2 == 0:
            for d in range(1, pairs):
                push(spot, spot, ds.at[kind, k, d], dr.at[kind, k, d],
                     seat.other_row(seat.row_behind(d)))
        push(spot, spot, cs.at[kind, k, 1], cr.at[kind, k, 1], seat.other_core())
        for d in range(1, pairs):
            spot = place(kind, seat.half, expert, seat.row_ahead(d) * 2 + seat.core)
            landed(spot, ys.at[kind, k, d], yr.at[kind, k, d])
            if k % 2 == 1:
                push(spot, spot, ds.at[kind, k, d], dr.at[kind, k, d], seat.other_half())
            push(spot, spot, cs.at[kind, k, 2 * d], cr.at[kind, k, 2 * d], seat.other_core())

    def third(kind, k):
        for d in range(1, pairs):
            spot = place(kind, 1 - seat.half, seat.ahead(offs[k]),
                         seat.row_ahead(d) * 2 + seat.core)
            landed(spot, ds.at[kind, k, d], dr.at[kind, k, d])
            push(spot, spot, cs.at[kind, k, 2 * d + 1], cr.at[kind, k, 2 * d + 1],
                 seat.other_core())

    for n in range(len(items) + 2):
        if n < len(items):
            first(*items[n])
        if 1 <= n <= len(items):
            second(*items[n - 1])
        if n >= 2:
            third(*items[n - 2])
    for kind, k in items:
        expert = seat.ahead(offs[k])
        for d in range(pairs):
            tp = seat.row_ahead(d) * 2 + 1 - seat.core
            for swap in range(2):
                half = seat.half if swap == 0 else 1 - seat.half
                landed(place(kind, half, expert, tp),
                       cs.at[kind, k, 2 * d + swap], cr.at[kind, k, 2 * d + swap])
    landed(early_ref, hs.at[0], hr.at[0])
    for copy in started:
        copy.wait_send()
    for copy in local:
        copy.wait()


def return_kernel(experts, pairs, part_ref, sel_ref, cot_hbm, conv_ref, sum_ref, outer_ref,
                  inner_ref, input_ref, taps_ref, weight_hbm,
                  rows_ref, routed_ref, hidden_ref, gate_ref, up_ref,
                  gate_grad_ref, up_grad_ref, down_grad_ref, out_grad_ref, outer_grad_ref, inner_grad_ref, input_grad_ref,
                  cot_ref, weight_ref, sg_ref, g_ref, c_ref, ext_ref, late_ref, a_ref, acc_ref, b1_ref, acc2_ref, b2_ref, fin_ref, ret_ref,
                  as_, ar, b1s, b1r, b2s, b2r, zs, zr, ms, mr, gs, gr, vs, vr, us, ur, hs, hr, own):
    seat = Seat(experts, pairs)
    capacity = part_ref.shape[2]
    width = part_ref.shape[3] // (2 * pairs)
    slice_width = g_ref.shape[3]
    offs = near_first(experts)
    order = list(reversed(range(experts)))
    sp_peers = [
        (expert * 2 + half, seat.tp)
        for d in range(experts)
        for expert in [seat.ahead(d)]
        for half in ([seat.half, 1 - seat.half] if d else [1 - seat.half])
    ]
    greet(
        sp_peers + [seat.other_core()]
        + [seat.other_row(seat.row_ahead(d)) for d in range(1, pairs)]
    )()
    started = []
    over_first = (((0,), (0,)), ((), ()))
    step = 512 if rows_ref.shape[1] % 512 == 0 else rows_ref.shape[1]
    pieces = [(n, at) for n in range(3) for at in range(0, rows_ref.shape[1], step)]

    def work(count):
        for n, at in [pieces.pop(0) for _ in range(min(count, len(pieces)))]:
            span = slice(at, at + step)
            if n < 2:
                delta, out = ((gate_ref, gate_grad_ref), (up_ref, up_grad_ref))[n]
                out[span, :] = lax.dot_general(
                    rows_ref[:, span], delta[...], over_first,
                    preferred_element_type=jnp.float32,
                ).astype(jnp.bfloat16)
            else:
                down_grad_ref[:, span] = lax.dot_general(
                    hidden_ref[...], routed_ref[:, span], over_first,
                    preferred_element_type=jnp.float32,
                ).astype(jnp.bfloat16)

    def cols(tp):
        return pl.ds(pl.multiple_of(tp * width, width), width)

    def push(src, dst, sent, landed, device):
        copy = remote(src, dst, sent, landed, device)
        copy.start()
        started.append(copy)

    def landed(spot, sem_s, sem_r):
        remote(spot, spot, sem_s, sem_r, seat.other_core()).wait_recv()

    def total(*terms):
        value = terms[0].astype(jnp.float32)
        for term in terms[1:]:
            value = value + term.astype(jnp.float32)
        return value.astype(jnp.bfloat16)

    def zone(k):
        return seat.behind(offs[k])

    for k in order:
        for half in range(2):
            for row in range(pairs):
                push(part_ref.at[half, zone(k), :, cols(row * 2 + 1 - seat.core)],
                     a_ref.at[half, row, k], as_.at[half, row, k], ar.at[half, row, k],
                     seat.other_core())
    copy_conv = pltpu.make_async_copy(conv_ref, c_ref.at[seat.half, seat.expert], own.at[0])
    copy_conv.start()
    mine = cols(seat.tp)
    load_cot = pltpu.make_async_copy(cot_hbm.at[:, mine], cot_ref, own.at[2])
    load_weight = pltpu.make_async_copy(weight_hbm, weight_ref, own.at[3])
    load_cot.start()
    load_weight.start()
    for k in range(1, experts):
        push(conv_ref, c_ref.at[seat.half, seat.expert], vs.at[k], vr.at[k],
             seat.other_expert(seat.behind(offs[k])))

    def first(k):
        for half in range(2):
            for row in range(pairs):
                landed(a_ref.at[half, row, k], as_.at[half, row, k], ar.at[half, row, k])
                acc_ref[half, row, k] = total(
                    part_ref[half, zone(k), :, cols(row * 2 + seat.core)], a_ref[half, row, k]
                )
        if k % 2 == 0:
            for row in range(pairs):
                push(acc_ref.at[1 - seat.half, row, k], b1_ref.at[k, row],
                     b1s.at[k, row], b1r.at[k, row], seat.other_half())
        else:
            for d in range(1, pairs):
                target = seat.row_behind(d)
                for half in range(2):
                    slot = 2 * (d - 1) + half
                    push(acc_ref.at[half, target, k], b1_ref.at[k, slot],
                         b1s.at[k, slot], b1r.at[k, slot], seat.other_row(target))

    def second(k):
        if k % 2 == 0:
            for row in range(pairs):
                landed(b1_ref.at[k, row], b1s.at[k, row], b1r.at[k, row])
                acc2_ref[k, row] = total(acc_ref[seat.half, row, k], b1_ref[k, row])
            for d in range(1, pairs):
                target = seat.row_behind(d)
                push(acc2_ref.at[k, target], b2_ref.at[k, d - 1], b2s.at[k, d - 1],
                     b2r.at[k, d - 1], seat.other_row(target))
        else:
            for half in range(2):
                terms = [acc_ref[half, seat.row, k]]
                for d in range(1, pairs):
                    slot = 2 * (d - 1) + half
                    landed(b1_ref.at[k, slot], b1s.at[k, slot], b1r.at[k, slot])
                    terms.append(b1_ref[k, slot])
                acc2_ref[k, half] = total(*terms)
            push(acc2_ref.at[k, 1 - seat.half], b2_ref.at[k, 0], b2s.at[k, 0], b2r.at[k, 0],
                 seat.other_half())

    def third(k):
        count = pairs - 1 if k % 2 == 0 else 1
        terms = [acc2_ref[k, seat.row if k % 2 == 0 else seat.half]]
        for slot in range(count):
            landed(b2_ref.at[k, slot], b2s.at[k, slot], b2r.at[k, slot])
            terms.append(b2_ref[k, slot])
        rows = pl.ds(pl.multiple_of(seat.expert * capacity, 16), capacity)
        if k == 0:
            ret_ref[rows, :] = total(*terms)
        else:
            fin_ref[k] = total(*terms)
            push(fin_ref.at[k], ret_ref.at[rows, :], zs.at[k], zr.at[k],
                 seat.other_expert(zone(k)))

    for n in range(experts + 2):
        if n < experts:
            first(order[n])
        work(1)
        if 1 <= n <= experts:
            second(order[n - 1])
        if n >= 2:
            third(order[n - 2])
    copy_conv.wait()
    for k in range(experts):
        expert = seat.ahead(offs[k])
        spot = c_ref.at[seat.half, expert]
        if k:
            landed(spot, vs.at[k], vr.at[k])
        push(spot, spot, us.at[k], ur.at[k], seat.other_half())
    work(2)
    load_cot.wait()
    load_weight.wait()
    for k in range(1, experts):
        rows = pl.ds(pl.multiple_of(seat.ahead(offs[k]) * capacity, 16), capacity)
        landed(ret_ref.at[rows, :], zs.at[k], zr.at[k])
    moe = lax.dot_general(
        sel_ref[...], ret_ref[...], over_first, preferred_element_type=jnp.float32
    )
    sg_ref[:, mine] = total(cot_ref[...], moe.astype(jnp.bfloat16))
    for d in range(1, pairs):
        push(sg_ref.at[:, mine], sg_ref.at[:, mine], ms.at[2 * d], mr.at[2 * d],
             seat.other_row(seat.row_behind(d)))
    push(sg_ref.at[:, mine], sg_ref.at[:, mine], ms.at[0], mr.at[0], seat.other_core())
    work(2)
    for d in range(1, pairs):
        theirs = sg_ref.at[:, cols(seat.row_ahead(d) * 2 + seat.core)]
        landed(theirs, ms.at[2 * d], mr.at[2 * d])
        push(theirs, theirs, ms.at[2 * d + 1], mr.at[2 * d + 1], seat.other_core())
    for d in range(pairs):
        slot = 0 if d == 0 else 2 * d + 1
        theirs = sg_ref.at[:, cols(seat.row_ahead(d) * 2 + 1 - seat.core)]
        landed(theirs, ms.at[slot], mr.at[slot])

    def piece(sp):
        return sg_ref.at[:, pl.ds(pl.multiple_of(sp * slice_width, 128), slice_width)]

    for k in range(experts):
        expert = seat.behind(offs[k])
        for swap in range(2):
            if k == 0 and swap == 0:
                continue
            half = seat.half if swap == 0 else 1 - seat.half
            push(piece(expert * 2 + half), g_ref.at[seat.half, seat.expert],
                 gs.at[k, swap], gr.at[k, swap], (expert * 2 + half, seat.tp))
    keep = pltpu.make_async_copy(piece(seat.sp), g_ref.at[seat.half, seat.expert], own.at[1])
    keep.start()
    tokens = sum_ref.shape[0]
    border = late_ref.shape[0]
    conv_grad = jnp.dot(sg_ref[...], weight_ref[...], preferred_element_type=jnp.float32)
    ext_ref[0:tokens, :] = conv_grad * outer_ref[...].astype(jnp.float32)
    push(ext_ref.at[0:border, :], late_ref, hs.at[0], hr.at[0], seat.next_tokens(-1))
    outer_grad_ref[...] = (conv_grad * sum_ref[...]).astype(jnp.bfloat16)
    keep.wait()
    out_grad_ref[...] = jnp.zeros_like(out_grad_ref)

    def add_out(half, expert):
        out_grad_ref[...] += lax.dot_general(
            g_ref[half, expert], c_ref[half, expert], over_first,
            preferred_element_type=jnp.float32,
        )

    add_out(seat.half, seat.expert)
    work(len(pieces))
    landed(late_ref, hs.at[0], hr.at[0])
    ext_ref[tokens:tokens + border, :] = jnp.where(
        seat.sp == 2 * experts - 1, 0.0, late_ref[...]
    )
    mixed_grad = taps_ref[2:3, :] * ext_ref[0:tokens, :]
    mixed_grad = mixed_grad + taps_ref[1:2, :] * ext_ref[1:tokens + 1, :]
    mixed_grad = mixed_grad + taps_ref[0:1, :] * ext_ref[2:tokens + 2, :]
    inner_grad_ref[...] = (mixed_grad * input_ref[...].astype(jnp.float32)).astype(jnp.bfloat16)
    input_grad_ref[...] = (mixed_grad * inner_ref[...].astype(jnp.float32)).astype(jnp.bfloat16)
    for k in range(experts):
        expert = seat.ahead(offs[k])
        landed(c_ref.at[1 - seat.half, expert], us.at[k], ur.at[k])
        for swap in range(2):
            if k == 0 and swap == 0:
                continue
            half = seat.half if swap == 0 else 1 - seat.half
            landed(g_ref.at[half, expert], gs.at[k, swap], gr.at[k, swap])
            add_out(half, expert)
    for copy in started:
        copy.wait_send()


def vmem(count):
    return [pl.BlockSpec(memory_space=pltpu.VMEM)] * count


def hbm(count):
    return [pl.BlockSpec(memory_space=pltpu.HBM)] * count


def sems(*shape):
    return pltpu.SemaphoreType.DMA(shape)


def dispatch(routes, route_weights, stream, cotangent, inner, given, capacity, experts, tp_count):
    pairs = tp_count // 2
    tokens, model_width = stream.shape
    width = model_width // tp_count
    border = min(16, tokens)
    shape = jax.ShapeDtypeStruct((2, experts, capacity, model_width), jnp.bfloat16)
    halo = (border, inner.shape[1])
    flat, rowed = (2, experts), (2, experts, pairs)
    cored = (2, experts, 2 * pairs)
    return pl.pallas_call(
        functools.partial(dispatch_kernel, experts, pairs),
        out_shape=(
            shape,
            shape,
            jax.ShapeDtypeStruct((experts * capacity, tokens), jnp.bfloat16),
            jax.ShapeDtypeStruct(halo, jnp.float32),
        ),
        in_specs=hbm(6),
        out_specs=tuple(vmem(4)),
        scratch_shapes=[
            pltpu.VMEM((2, experts, capacity, width), jnp.bfloat16),
            pltpu.VMEM(halo, jnp.float32),
            pltpu.VMEM((2, tokens), jnp.int32),
            pltpu.VMEM((2, tokens), jnp.float32),
            pltpu.VMEM((2, tokens, width), jnp.bfloat16),
            pltpu.VMEM((2,) + halo, jnp.bfloat16),
        ]
        + [
            sems(*s)
            for s in (
                flat, flat, flat, flat, rowed, rowed, rowed, rowed, cored, cored,
                (2,), (1,), (1,), (6,),
            )
        ],
        compiler_params=pltpu.CompilerParams(
            collective_id=0, has_side_effects=True, vmem_limit_bytes=12 * 1024 * 1024
        ),
    )(routes.T, route_weights.T, stream, cotangent, inner, given)


def give_back(part, select, cotangent, conv_out, conv_sum, outer, inner, given, taps,
              out_weight, rows, routed, hidden, gate_delta, up_delta, experts, tp_count):
    pairs = tp_count // 2
    _, _, capacity, model_width = part.shape
    tokens, channels = conv_out.shape
    width = model_width // tp_count
    slice_width = model_width // (2 * experts)
    border = min(8, tokens)
    most = max(pairs, 2 * (pairs - 1))
    late = max(pairs - 1, 1)
    bf16 = jnp.bfloat16
    units = hidden.shape[1]
    gate_shape = jax.ShapeDtypeStruct((model_width, units), bf16)
    own_channels = jax.ShapeDtypeStruct((tokens, channels), bf16)
    return pl.pallas_call(
        functools.partial(return_kernel, experts, pairs),
        out_shape=(
            gate_shape,
            gate_shape,
            jax.ShapeDtypeStruct((units, model_width), bf16),
            jax.ShapeDtypeStruct((slice_width, channels), jnp.float32),
            own_channels,
            own_channels,
            own_channels,
        ),
        in_specs=vmem(2) + hbm(1) + vmem(6) + hbm(1) + vmem(5),
        out_specs=tuple(vmem(7)),
        scratch_shapes=[
            pltpu.VMEM((tokens, width), bf16),
            pltpu.VMEM((model_width, channels), bf16),
            pltpu.VMEM((tokens, model_width), bf16),
            pltpu.VMEM((2, experts, tokens, slice_width), bf16),
            pltpu.VMEM((2, experts, tokens, channels), bf16),
            pltpu.VMEM((tokens + border, channels), jnp.float32),
            pltpu.VMEM((border, channels), jnp.float32),
            pltpu.VMEM((2, pairs, experts, capacity, width), bf16),
            pltpu.VMEM((2, pairs, experts, capacity, width), bf16),
            pltpu.VMEM((experts, most, capacity, width), bf16),
            pltpu.VMEM((experts, max(pairs, 2), capacity, width), bf16),
            pltpu.VMEM((experts, late, capacity, width), bf16),
            pltpu.VMEM((experts, capacity, width), bf16),
            pltpu.VMEM((experts * capacity, width), bf16),
        ]
        + [
            sems(*s)
            for shape in (
                (2, pairs, experts), (experts, most), (experts, late), (experts,),
                (2 * pairs,), (experts, 2), (experts,), (experts,), (1,),
            )
            for s in (shape, shape)
        ]
        + [sems(4)],
        compiler_params=pltpu.CompilerParams(
            collective_id=1, has_side_effects=True, vmem_limit_bytes=18 * 1024 * 1024
        ),
    )(
        part, select, cotangent, conv_out, conv_sum, outer, inner, given, taps, out_weight,
        rows, routed, hidden, gate_delta, up_delta,
    )


def per_device(
    cotangent,
    stream,
    routes,
    route_weights,
    gate_weight,
    up_weight,
    down_weight,
    outer_gate,
    inner_gate,
    conv_input,
    conv_taps,
    out_weight,
):
    groups = lax.axis_size("sp")
    tp_count = lax.axis_size("tp")
    experts = groups // 2
    tok_rows = stream.shape[0]
    model_width = stream.shape[1]
    capacity = 3 * tok_rows // experts
    slot_total = experts * capacity
    contract_first = (((0,), (0,)), ((), ()))
    contract_last = (((1,), (1,)), ((), ()))
    block_width = model_width // tp_count
    slots = groups * capacity
    direct = tp_count % 2 == 0 and capacity % 16 == 0 and block_width % 128 == 0
    taps = conv_taps.astype(jnp.float32)
    outer_f = outer_gate.astype(jnp.float32)
    inner_f = inner_gate.astype(jnp.float32)
    input_f = conv_input.astype(jnp.float32)
    mixed = inner_f * input_f
    if direct:
        routed_rows, routed_cot, select, early = dispatch(
            routes, route_weights, stream, cotangent, inner_gate, conv_input,
            capacity, experts, tp_count,
        )
        routed_rows = routed_rows.reshape(slots, model_width)
        routed_cot = routed_cot.reshape(slots, model_width)
        earlier = jnp.where(lax.axis_index("sp") == 0, 0.0, early[-2:])
    else:
        flat_routes = routes.reshape(-1)
        choose = (flat_routes[:, None] == jnp.arange(experts, dtype=jnp.int32)[None, :]).astype(
            jnp.int32
        )
        before = jnp.cumsum(choose, axis=0) - choose
        slot_place = flat_routes * capacity + jnp.sum(before * choose, axis=1)
        slot_table = (jnp.arange(slot_total, dtype=jnp.int32)[:, None] == slot_place[None, :]).astype(
            jnp.float32
        )
        select = jnp.sum(slot_table.reshape(slot_total, tok_rows, 2), axis=2).astype(jnp.bfloat16)
        slot_weight = jnp.sum(slot_table * route_weights.reshape(-1)[None, :], axis=1)
        offset = lax.axis_index("tp") * block_width
        rows_part = lax.dynamic_slice_in_dim(stream, offset, block_width, 1)
        cot_part = lax.dynamic_slice_in_dim(cotangent, offset, block_width, 1)
        sent_rows = jnp.dot(select, rows_part, preferred_element_type=jnp.float32).astype(jnp.bfloat16)
        sent_cot = (
            jnp.dot(select, cot_part, preferred_element_type=jnp.float32) * slot_weight[:, None]
        ).astype(jnp.bfloat16)
        sent_rows = jnp.repeat(sent_rows.reshape(experts, capacity, -1), 2, axis=0)
        sent_cot = jnp.repeat(sent_cot.reshape(experts, capacity, -1), 2, axis=0)
        recv_rows, recv_cot = (
            lax.all_to_all(sent_rows, "sp", split_axis=0, concat_axis=0, tiled=True),
            lax.all_to_all(sent_cot, "sp", split_axis=0, concat_axis=0, tiled=True),
        )
        recv_rows, recv_cot = (
            lax.all_gather(recv_rows, "tp", axis=2, tiled=True),
            lax.all_gather(recv_cot, "tp", axis=2, tiled=True),
        )
        routed_rows = recv_rows.reshape(slots, model_width)
        routed_cot = recv_cot.reshape(slots, model_width)
        earlier = from_behind(mixed[-2:], "sp", 1)
    gate_local = gate_weight[0]
    up_local = up_weight[0]
    down_local = down_weight[0]
    gate_pre = jnp.dot(routed_rows, gate_local, preferred_element_type=jnp.float32)
    up_pre = jnp.dot(routed_rows, up_local, preferred_element_type=jnp.float32)
    hidden_grad = lax.dot_general(
        routed_cot, down_local, contract_last, preferred_element_type=jnp.float32
    )
    sigma = jax.nn.sigmoid(gate_pre)
    silu_gate = gate_pre * sigma
    hidden = (silu_gate * up_pre).astype(jnp.bfloat16)
    up_delta = (hidden_grad * silu_gate).astype(jnp.bfloat16)
    gate_delta = (hidden_grad * up_pre * sigma * (1.0 + gate_pre * (1.0 - sigma))).astype(
        jnp.bfloat16
    )
    row_partial = lax.dot_general(
        gate_delta, gate_local, contract_last, preferred_element_type=jnp.float32
    )
    row_partial = row_partial + lax.dot_general(
        up_delta, up_local, contract_last, preferred_element_type=jnp.float32
    )
    padded = jnp.concatenate([earlier, mixed], axis=0)
    conv_sum = taps[0] * padded[:-2] + taps[1] * padded[1:-1] + taps[2] * padded[2:]
    conv_out = (outer_f * conv_sum).astype(jnp.bfloat16)
    if direct:
        gate_grad, up_grad, down_grad, out_grad, outer_grad, inner_grad, input_grad = give_back(
            row_partial.astype(jnp.bfloat16).reshape(2, experts, capacity, model_width),
            select,
            cotangent,
            conv_out,
            conv_sum,
            outer_gate,
            inner_gate,
            conv_input,
            taps,
            out_weight,
            routed_rows,
            routed_cot,
            hidden,
            gate_delta,
            up_delta,
            experts,
            tp_count,
        )
        gate_grad, up_grad, down_grad = gate_grad[None], up_grad[None], down_grad[None]
    else:
        gate_grad = lax.dot_general(
            routed_rows, gate_delta, contract_first, preferred_element_type=jnp.float32
        ).astype(jnp.bfloat16)[None]
        up_grad = lax.dot_general(
            routed_rows, up_delta, contract_first, preferred_element_type=jnp.float32
        ).astype(jnp.bfloat16)[None]
        down_grad = lax.dot_general(
            hidden, routed_cot, contract_first, preferred_element_type=jnp.float32
        ).astype(jnp.bfloat16)[None]
        half_sums = lax.psum_scatter(
            row_partial.astype(jnp.bfloat16), "tp", scatter_dimension=1, tiled=True
        ).astype(jnp.float32)
        block_width = half_sums.shape[1]
        half_grad = half_sums.reshape(groups, capacity, block_width).astype(jnp.bfloat16)
        returned = lax.all_to_all(half_grad, "sp", split_axis=0, concat_axis=0, tiled=True)
        returned = returned.reshape(experts, 2, capacity, block_width)
        select_three = select.reshape(experts, capacity, tok_rows)
        moe_part = jnp.einsum(
            "ecr,emcd->rd", select_three, returned, preferred_element_type=jnp.float32
        ).astype(jnp.bfloat16)
        moe_grad = lax.all_gather(moe_part, "tp", axis=1, tiled=True)
        stream_grad = (cotangent.astype(jnp.float32) + moe_grad.astype(jnp.float32)).astype(
            jnp.bfloat16
        )
        out_grad = lax.psum_scatter(
            lax.dot_general(
                stream_grad, conv_out, contract_first, preferred_element_type=jnp.float32
            ).astype(jnp.bfloat16),
            "sp",
            scatter_dimension=0,
            tiled=True,
        ).astype(jnp.float32)
        conv_grad = jnp.dot(stream_grad, out_weight, preferred_element_type=jnp.float32)
        outer_grad = (conv_grad * conv_sum).astype(jnp.bfloat16)
        scaled = conv_grad * outer_f
        later = from_behind(scaled[:2], "sp", -1)
        extended = jnp.concatenate([scaled, later], axis=0)
        mixed_grad = taps[2] * extended[:-2] + taps[1] * extended[1:-1] + taps[0] * extended[2:]
        inner_grad = (mixed_grad * input_f).astype(jnp.bfloat16)
        input_grad = (mixed_grad * inner_f).astype(jnp.bfloat16)
    return (gate_grad, up_grad, down_grad, out_grad, outer_grad, inner_grad, input_grad)


def solution(mesh):
    placed = (
        P("sp", None),
        P("sp", None),
        P("sp", None),
        P("sp", None),
        P("sp", None, "tp"),
        P("sp", None, "tp"),
        P("sp", "tp", None),
        P("sp", "tp"),
        P("sp", "tp"),
        P("sp", "tp"),
        P(None, "tp"),
        P(None, "tp"),
    )
    return jax.shard_map(
        per_device,
        mesh=mesh,
        in_specs=placed,
        out_specs=(
            P("sp", None, "tp"),
            P("sp", None, "tp"),
            P("sp", "tp", None),
            P("sp", "tp"),
            P("sp", "tp"),
            P("sp", "tp"),
            P("sp", "tp"),
        ),
        check_vma=False,
    )
```

profile of v0, /device:TPU:5, one launch (start us, length us, event | category | flops | bytes accessed | tf_op | source)
XLA Modules:
  0.0 113.0 jit_solution(10959293795886815342)
XLA Ops:
  0.6 0.0 copy-start
  0.7 0.9 fusion.16
  1.5 0.7 convert_element_type.31.taps_ref
  2.2 0.9 convert_multiply_fusion
  3.1 0.0 copy-start.1
  3.1 1.0 copy-done.1
  4.1 0.0 copy-start.4
  4.1 0.8 copy-done.4
  5.0 0.0 copy-start.6
  5.0 0.8 copy-done.6
  5.8 0.0 copy-start.8
  5.8 1.0 copy-done.8
  6.9 0.0 copy-start.10
  6.9 0.7 copy-done.10
  7.5 0.0 copy-start.11
  7.5 0.7 copy-done.11
  8.2 40.9 %shard_map.171 = (bf16[2,4,96,2048]{3,2,1,0:T(8,128)(2,1)S(1)}, bf16[2,4,96,2048]{3,2,1,0:T(8,128)(2,1)S(1)}, bf16[384,128]{1,0:T(8,128)(2,1)S(1)}, f32[16,256]{1,0:T(8,128)S(1)}) custom-call(s32[2,128]{1,0:T(2,128)S(1)} %bitcast.40, f32[2,128]{1,0:T(2,128)S(1)} %bitcast.41, bf16[128,2048]{1,0:T(8,128)(2,1)S(1)} %copy-done.8, ...), custom_call_target="tpu_custom_call" | custom-call | tf_op jit(solution)/shard_map/pallas_call | solution.py:477
  49.1 0.9 multiply_convert_fusion.3
  50.0 0.0 copy-start.12
  50.0 3.6 %fusion.7 = f32[768,512]{1,0:T(8,128)S(1)} fusion(bf16[768,2048]{1,0:T(8,128)(2,1)S(1)} %bitcast.35, bf16[1,512,2048]{2,1,0:T(8,128)(2,1)} %param.18), kind=kOutput, calls=%fused_computation.8 | convolution fusion | flops 1610612736 | bytes 6815744 | tf_op jit(solution)/shard_map/dot_general | solution.py:645
  53.6 0.0 copy-done.12
  53.6 1.8 %fusion.2 = f32[768,512]{1,0:T(8,128)S(1)} fusion(bf16[768,2048]{1,0:T(8,128)(2,1)S(1)} %bitcast.32, bf16[1,2048,512]{2,1,0:T(8,128)(2,1)S(1)} %copy-done.12), kind=kOutput, calls=%fused_computation.3 | convolution fusion | flops 1610612736 | bytes 6815744 | tf_op jit(solution)/shard_map/dot_general | solution.py:643
  55.4 0.0 copy-done
  55.4 2.5 %multiply_convert_fusion = (bf16[768,512]{1,0:T(8,128)(2,1)S(1)}, bf16[768,512]{1,0:T(8,128)(2,1)S(1)}, bf16[768,512]{1,0:T(8,128)(2,1)S(1)}) fusion(f32[768,512]{1,0:T(8,128)S(1)} %fusion.2, f32[768,512]{1,0:T(8,128)S(1)} %fusion.7, bf16[768,2048]{1,0:T(8,128)(2,1)S(1)} %bitcast.33, bf16[1,2048,512]{2,1,0:T(8,128)(2,1)S(1)} %copy-done), kind=kOutput, calls=%fused_computation.10 | convolution fusion | flops 1616510976 | bytes 10747904 | tf_op jit(solution)/shard_map/dot_general | solution.py:644
  57.9 1.8 %fusion = f32[768,2048]{1,0:T(8,128)S(1)} fusion(bf16[768,512]{1,0:T(8,128)(2,1)S(1)} %get-tuple-element.32.gate_ref, bf16[1,2048,512]{2,1,0:T(8,128)(2,1)S(1)} %copy-done.12), kind=kOutput, calls=%fused_computation.1 | convolution fusion | flops 1610612736 | bytes 9175040 | tf_op jit(solution)/shard_map/dot_general | solution.py:655
  59.7 0.0 copy-start.2
  59.7 0.0 copy-start.3
  59.7 0.0 copy-start.5
  59.7 0.0 copy-start.7
  59.7 0.0 copy-start.9
  59.8 1.9 %add_convert_fusion = bf16[768,2048]{1,0:T(8,128)(2,1)S(1)} fusion(f32[768,2048]{1,0:T(8,128)S(1)} %fusion, bf16[768,512]{1,0:T(8,128)(2,1)S(1)} %get-tuple-element.33.up_ref, bf16[1,2048,512]{2,1,0:T(8,128)(2,1)S(1)} %copy-done), kind=kOutput, calls=%fused_computation | convolution fusion | flops 1613758464 | bytes 12320768 | tf_op jit(solution)/shard_map/dot_general | solution.py:658
  61.6 0.0 copy-done.2
  61.6 0.0 copy-done.3
  61.6 0.0 copy-done.5
  61.7 0.0 copy-done.7
  61.7 0.0 copy-done.9
  61.7 44.8 %shard_map.172 = (bf16[2048,512]{1,0:T(8,128)(2,1)S(1)}, bf16[2048,512]{1,0:T(8,128)(2,1)S(1)}, bf16[512,2048]{1,0:T(8,128)(2,1)S(1)}, f32[256,256]{1,0:T(8,128)...) custom-call(bf16[2,4,96,2048]{3,2,1,0:T(8,128)(2,1)S(1)} %bitcast.31, ...), custom_call_target="tpu_custom_call" | custom-call | tf_op jit(solution)/shard_map/pallas_call | solution.py:522
  106.4 1.3 %copy.26 = bf16[1,2048,512]{2,1,0:T(8,128)(2,1)} copy(bf16[1,2048,512]{2,1,0:T(8,128)(2,1)S(1)} %bitcast.39) | data formatting | bytes 4194304
  107.8 1.3 %copy.27 = bf16[1,2048,512]{2,1,0:T(8,128)(2,1)} copy(bf16[1,2048,512]{2,1,0:T(8,128)(2,1)S(1)} %bitcast.38) | data formatting | bytes 4194304
  109.1 1.3 %copy.28 = bf16[1,512,2048]{2,1,0:T(8,128)(2,1)} copy(bf16[1,512,2048]{2,1,0:T(8,128)(2,1)S(1)} %bitcast.37) | data formatting | bytes 4194304
  110.4 0.7 copy.29
  111.1 0.6 copy.30
  111.7 0.6 copy.31
  112.4 0.6 copy.32
  (1 shorter events, 0.0 us)
Async XLA Ops:
  0.6 54.8 %copy-start = (bf16[1,2048,512]{2,1,0:T(8,128)(2,1)S(1)}, bf16[1,2048,512]{2,1,0:T(8,128)(2,1)}, u32[]{:S(2)}) copy-start(bf16[1,2048,512]{2,1,0:T(8,128)(2,1)} %param.17) | copy-start | bytes 6291460
  3.1 1.0 copy-start.1
  4.1 0.8 copy-start.4
  5.0 0.8 copy-start.6
  5.8 1.0 copy-start.8
  6.9 0.7 copy-start.10
  7.5 0.7 copy-start.11
  50.0 3.6 %copy-start.12 = (bf16[1,2048,512]{2,1,0:T(8,128)(2,1)S(1)}, bf16[1,2048,512]{2,1,0:T(8,128)(2,1)}, u32[]{:S(2)}) copy-start(bf16[1,2048,512]{2,1,0:T(8,128)(2,1)} %param.16) | copy-start | bytes 6291460
  59.7 1.9 %copy-start.2 = (bf16[128,2048]{1,0:T(8,128)(2,1)S(1)}, bf16[128,2048]{1,0:T(8,128)(2,1)}, u32[]{:S(2)}) copy-start(bf16[128,2048]{1,0:T(8,128)(2,1)} %cot_hbm.1) | copy-start | bytes 1572868
  59.7 1.9 %copy-start.3 = (bf16[2048,256]{1,0:T(8,128)(2,1)S(1)}, bf16[2048,256]{1,0:T(8,128)(2,1)}, u32[]{:S(2)}) copy-start(bf16[2048,256]{1,0:T(8,128)(2,1)} %weight_hbm.1) | copy-start | bytes 3145732
  59.7 1.9 %copy-start.5 = (bf16[128,256]{1,0:T(8,128)(2,1)S(1)}, bf16[128,256]{1,0:T(8,128)(2,1)}, u32[]{:S(2)}) copy-start(bf16[128,256]{1,0:T(8,128)(2,1)} %inner_ref.1) | copy-start | bytes 196612
  59.7 1.9 %copy-start.7 = (bf16[128,256]{1,0:T(8,128)(2,1)S(1)}, bf16[128,256]{1,0:T(8,128)(2,1)}, u32[]{:S(2)}) copy-start(bf16[128,256]{1,0:T(8,128)(2,1)} %input_ref.1) | copy-start | bytes 196612
  59.7 1.9 %copy-start.9 = (bf16[128,256]{1,0:T(8,128)(2,1)S(1)}, bf16[128,256]{1,0:T(8,128)(2,1)}, u32[]{:S(2)}) copy-start(bf16[128,256]{1,0:T(8,128)(2,1)} %outer_ref.1) | copy-start | bytes 196612
where the time goes:
time: 115 us; the launch traced here: 113 us
  Pallas kernels  85.6 us (74%)
  local copies, waits for them, and re-layouts  12.6 us (11%)
  matrix products  11.5 us (10%)
  other arithmetic  2.48 us (2%)
    pallas_call x1, Pallas kernels, give_back(): pl.pallas_call(functools.partial(return_kernel, experts, pairs), out_shap...  44.8 us
    pallas_call x1, Pallas kernels, dispatch(): pl.pallas_call(functools.partial(dispatch_kernel, experts, pairs), out_sh...  40.9 us
    unnamed x33, local copies, waits for them, and re-layouts  11.7 us
    dot_general x1, matrix products, per_device(): lax.dot_general(routed_cot, down_local, contract_last, preferred_element_...  3.56 us
    dot_general x1, matrix products, per_device(): up_pre = jnp.dot(routed_rows, up_local, preferred_element_type=jnp.float32)  2.46 us

commit v1 on v0

v1 whole, which is shorter than its diff:
```python
import functools

import jax
import jax.numpy as jnp
from jax import lax
from jax.experimental import pallas as pl
from jax.experimental.pallas import tpu as pltpu
from jax.sharding import PartitionSpec as P


def from_behind(block, axis, distance):
    devices = range(lax.axis_size(axis))
    route = [(i - distance, i) for i in devices if i - distance in devices]
    return lax.ppermute(block, axis, route)


def remote(src, dst, sent, landed, device):
    return pltpu.make_async_remote_copy(
        src_ref=src,
        dst_ref=dst,
        send_sem=sent,
        recv_sem=landed,
        device_id=device,
        device_id_type=pl.DeviceIdType.MESH,
    )


class Seat:
    def __init__(self, experts):
        self.sp = lax.axis_index("sp")
        self.tp = lax.axis_index("tp")
        self.x = lax.rem(self.sp, 2)
        self.z = self.sp // 2
        self.c = lax.rem(self.tp, 2)
        self.y = self.tp // 2
        self.experts = experts

    def plane(self, k):
        number, weight = 0, 1
        while weight < self.experts:
            bit = lax.rem(self.z // weight, 2)
            number = number + weight * (1 - bit if k // weight % 2 else bit)
            weight *= 2
        return number

    def over_z(self, k, swap=0):
        return (self.plane(k) * 2 + (1 - self.x if swap else self.x), self.tp)

    def over_x(self):
        return (self.z * 2 + 1 - self.x, self.tp)

    def over_y(self):
        return (self.sp, (1 - self.y) * 2 + self.c)

    def other_core(self):
        return (self.sp, self.y * 2 + 1 - self.c)

    def next_tokens(self, distance):
        groups = 2 * self.experts
        return (lax.rem(self.sp + groups + distance, groups), self.tp)


SEMS = {
    "z": lambda n: (2, n), "x": lambda n: (2, n), "y": lambda n: (2, n), "d": lambda n: (2, n, 2),
    "c": lambda n: (2, n, 4), "r1": lambda n: (n, 2), "r2": lambda n: (n, 2),
    "r3": lambda n: (n, 2), "r4": lambda n: (n,), "ag": lambda n: (3,), "g": lambda n: (n, 2),
    "gc": lambda n: (n, 2), "cz": lambda n: (n,), "cx": lambda n: (n,), "h": lambda n: (2,),
}

FIRST = (((0,), (0,)), ((), ()))
LAST = (((1,), (1,)), ((), ()))


def fused_kernel(experts, capacity, *refs):
    refs = list(refs)

    def take(count):
        got = refs[:count]
        del refs[:count]
        return got

    (routes_hbm, weights_hbm, stream_hbm, given_hbm, gate_hbm, up_hbm, down_hbm, outer_hbm,
     inner_hbm, input_hbm, taps_hbm, ow_hbm) = take(12)
    (gate_grad, up_grad, down_grad, out_grad, outer_grad, inner_grad, input_grad) = take(7)
    (routes_ref, weights_ref, block, sel, slot_weight, gate, up, down, outer, inner, given, taps, ow,
     send, rows, cots, gp_ref, up_ref, hid, delta, part, mine_part, a_ref, acc, b1a, b1b, acc2a,
     acc2b, b2a, b2b, fin, ret, sg, g_ref, c_ref, sum_ref, tail_ref, early, ext,
     late) = take(40)
    load_sem, keep_sem = take(2)
    sem = {}
    for name in SEMS:
        sem[name] = take(2)
    seat = Seat(experts)
    n_k = experts
    tokens, model = block.shape[1:]
    width = send.shape[3]
    units = gate.shape[1]
    cut = capacity // 2 // 16 * 16
    places = (rows, cots)
    slots = 2 * capacity
    f32, bf16 = jnp.float32, jnp.bfloat16
    started = []

    barrier = pltpu.get_barrier_semaphore()
    peers = [seat.over_z(k, s) for k in range(n_k) for s in range(2) if k or s]
    peers += [seat.over_y(), seat.other_core()]

    pairs = (
        (routes_hbm, routes_ref), (weights_hbm, weights_ref), (stream_hbm, block.at[0]),
        (given_hbm, block.at[1]), (inner_hbm, inner), (input_hbm, given), (gate_hbm, gate),
        (up_hbm, up), (down_hbm, down), (outer_hbm, outer), (taps_hbm, taps), (ow_hbm, ow),
    )
    loads = [pltpu.make_async_copy(s, d, load_sem.at[n]) for n, (s, d) in enumerate(pairs)]
    for load in loads:
        load.start()
    for peer in peers:
        pl.semaphore_signal(barrier, inc=1, device_id=peer, device_id_type=pl.DeviceIdType.MESH)

    def push(src, dst, name, at, device):
        sent, got = sem[name]
        copy = remote(src, dst, sent.at[at], got.at[at], device)
        copy.start()
        started.append(copy)

    def landed(spot, name, at):
        sent, got = sem[name]
        remote(spot, spot, sent.at[at], got.at[at], seat.other_core()).wait_recv()

    def cols(tp):
        return pl.ds(pl.multiple_of(tp * width, width), width)

    def total(*terms):
        value = terms[0].astype(f32)
        for term in terms[1:]:
            value = value + term.astype(f32)
        return value.astype(bf16)

    my_cols = cols(seat.tp)
    y_cols = cols((1 - seat.y) * 2 + seat.c)
    core_cols = [cols(seat.y * 2 + 1 - seat.c), cols((1 - seat.y) * 2 + 1 - seat.c)]

    tail_rows = tail_ref.shape[0]
    edge = slice(tokens - tail_rows, tokens)

    def send_halo():
        loads[4].wait()
        loads[5].wait()
        tail_ref[...] = inner[edge, :].astype(f32) * given[edge, :].astype(f32)
        pl.semaphore_wait(barrier, len(peers))
        push(tail_ref, early, "h", 0, seat.next_tokens(1))

    loads[0].wait()
    loads[1].wait()
    place_of = lax.broadcasted_iota(jnp.int32, (n_k, tokens), 0)
    number = jnp.zeros((n_k, tokens), jnp.int32)
    for k in range(n_k):
        number = jnp.where(place_of == k, seat.plane(k), number)
    named = [routes_ref[j:j + 1, :] == number for j in range(2)]
    member = jnp.where(named[0] | named[1], 1.0, 0.0)
    share = jnp.where(named[0], weights_ref[0:1, :], 0.0) + jnp.where(
        named[1], weights_ref[1:2, :], 0.0
    )
    sooner = lax.broadcasted_iota(jnp.int32, (tokens, tokens), 0) < lax.broadcasted_iota(
        jnp.int32, (tokens, tokens), 1
    )
    rank = jnp.dot(
        member.astype(bf16), jnp.where(sooner, 1.0, 0.0).astype(bf16), preferred_element_type=f32
    )
    slot = lax.broadcasted_iota(jnp.int32, (capacity, tokens), 0).astype(f32)
    for k in range(n_k):
        chosen = jnp.where(slot == rank[k:k + 1], member[k:k + 1], 0.0)
        slot_weight[k] = jnp.sum(chosen * share[k:k + 1], axis=1, keepdims=True)
        sel[k * capacity:(k + 1) * capacity, :] = chosen.astype(bf16)

    def pick(kind, k, span):
        got = jnp.dot(
            sel[k * capacity:(k + 1) * capacity, :], block[kind, :, span],
            preferred_element_type=f32,
        )
        if kind:
            got = got * slot_weight[k]
        return got.astype(bf16)

    order = list(range(n_k))

    def fill(k, kind):
        if k == order[1]:
            loads[2 + kind].wait()
        send[kind, k] = pick(kind, k, my_cols)
        if k == order[1] and kind == 0:
            send_halo()
        push(send.at[kind, k], places[kind].at[k, seat.x, :, my_cols], "z", (kind, k),
             seat.over_z(k))

    for k in order[1:]:
        for kind in range(2):
            fill(k, kind)

    def spot_of(item, x, span):
        kind, k = item
        return places[kind].at[k, x, :, span]

    def half_of(item, x, span, j):
        kind, k = item
        return places[kind].at[k, x, pl.ds(cut, capacity - cut) if j else pl.ds(0, cut), span]

    ox = 1 - seat.x

    def s1(item):
        kind, k = item
        if k == 0:
            for tp in range(model // width):
                span = slice(tp * width, (tp + 1) * width)
                places[kind][0, seat.x, :, span] = pick(kind, 0, span)
            spot = spot_of(item, seat.x, my_cols)
            push(spot, spot, "x", item, seat.over_x())
        else:
            spot = spot_of(item, seat.x, my_cols)
            landed(spot, "z", item)
            push(spot, spot, "x", item, seat.over_x())
            push(spot, spot, "y", item, seat.over_y())
            push(spot, spot, "c", item + (0,), seat.other_core())

    def s2(item):
        kind, k = item
        spot = spot_of(item, ox, my_cols)
        landed(spot, "x", item)
        if k == 0:
            push(spot, spot, "y", item, seat.over_y())
        else:
            part_spot = half_of(item, ox, my_cols, 0)
            push(part_spot, part_spot, "d", item + (0,), seat.over_y())
        push(spot, spot, "c", item + (1,), seat.other_core())
        if k:
            spot = spot_of(item, seat.x, y_cols)
            landed(spot, "y", item)
            part_spot = half_of(item, seat.x, y_cols, 1)
            push(part_spot, part_spot, "d", item + (1,), seat.over_x())
            push(spot, spot, "c", item + (2,), seat.other_core())

    def s3(item):
        kind, k = item
        spot = spot_of(item, ox, y_cols)
        if k == 0:
            landed(spot, "y", item)
        else:
            landed(half_of(item, ox, y_cols, 0), "d", item + (0,))
            landed(half_of(item, ox, y_cols, 1), "d", item + (1,))
        push(spot, spot, "c", item + (3,), seat.other_core())

    def s4(item):
        kind, k = item
        for j in range(4):
            if k == 0 and j % 2 == 0:
                continue
            landed(spot_of(item, ox if j % 2 else seat.x, core_cols[j // 2]), "c", item + (j,))

    tile = 256 if units % 256 == 0 else units

    def pre(k):
        lhs = rows[k].reshape(slots, model)
        for at in range(0, units, tile):
            gp_ref[:, at:at + tile] = jnp.dot(lhs, gate[:, at:at + tile], preferred_element_type=f32)
            up_ref[:, at:at + tile] = jnp.dot(lhs, up[:, at:at + tile], preferred_element_type=f32)

    def mid(k):
        lhs = cots[k].reshape(slots, model)
        for at in range(0, units, tile):
            span = slice(at, at + tile)
            grad = lax.dot_general(lhs, down[span, :], LAST, preferred_element_type=f32)
            gate_pre, up_pre = gp_ref[:, span], up_ref[:, span]
            sigma = jax.nn.sigmoid(gate_pre)
            silu = gate_pre * sigma
            hid[k, :, span] = (silu * up_pre).astype(bf16)
            delta[k, :, units + at:units + at + tile] = (grad * silu).astype(bf16)
            delta[k, :, span] = (grad * up_pre * sigma * (1.0 + gate_pre * (1.0 - sigma))).astype(bf16)

    def post(k, y, mine):
        out = mine_part if mine else part
        core = seat.c if mine else 1 - seat.c
        for at in range(0, width, tile):
            first = pl.ds(pl.multiple_of((y * 2 + core) * width + at, tile), tile)
            value = lax.dot_general(
                delta[k, :, :units], gate[first, :], LAST, preferred_element_type=f32
            )
            value = value + lax.dot_general(
                delta[k, :, units:], up[first, :], LAST, preferred_element_type=f32
            )
            out[k, y, :, :, at:at + tile] = value.astype(bf16).reshape(2, capacity, tile)
        if not mine:
            push(part.at[k, y], a_ref.at[k, y], "r1", (k, y), seat.other_core())

    def r2(k):
        for y in range(2):
            landed(a_ref.at[k, y], "r1", (k, y))
            acc[k, y] = total(mine_part[k, y], a_ref[k, y])
        push(acc.at[k, :, ox, pl.ds(0, cut), :], b1a.at[k], "r2", (k, 0), seat.over_x())
        push(acc.at[k, 1 - seat.y, :, pl.ds(cut, capacity - cut), :], b1b.at[k], "r2", (k, 1),
             seat.over_y())

    def r3(k):
        landed(b1a.at[k], "r2", (k, 0))
        for y in range(2):
            acc2a[k, y] = total(acc[k, y, seat.x, 0:cut, :], b1a[k, y])
        push(acc2a.at[k, 1 - seat.y], b2a.at[k], "r3", (k, 0), seat.over_y())
        landed(b1b.at[k], "r2", (k, 1))
        for x in range(2):
            acc2b[k, x] = total(acc[k, seat.y, x, cut:capacity, :], b1b[k, x])
        push(acc2b.at[k, ox], b2b.at[k], "r3", (k, 1), seat.over_x())

    def r4(k):
        landed(b2a.at[k], "r3", (k, 0))
        landed(b2b.at[k], "r3", (k, 1))
        out = fin.at[k] if k else ret.at[0]
        out[0:cut, :] = total(acc2a[k, seat.y], b2a[k])
        out[cut:capacity, :] = total(acc2b[k, seat.x], b2b[k])
        if k:
            push(fin.at[k], ret.at[k], "r4", (k,), seat.over_z(k))

    step = 256 if model % 256 == 0 else model
    pieces = [(0, at) for at in range(0, model, step)] + [(1, at) for at in range(0, model, 2 * step)]

    def work(count):
        for _ in range(min(count, len(pieces))):
            kind, at = pieces.pop(0)
            if kind == 0:
                lhs = rows[:, :, :, at:at + step].reshape(n_k * slots, step)
                for half in range(2):
                    out = up_grad if half else gate_grad
                    out[at:at + step, :] = lax.dot_general(
                        lhs, delta[:, :, half * units:(half + 1) * units].reshape(n_k * slots, units),
                        FIRST, preferred_element_type=f32,
                    ).astype(bf16)
            else:
                rhs = cots[:, :, :, at:at + 2 * step].reshape(n_k * slots, 2 * step)
                down_grad[:, at:at + 2 * step] = lax.dot_general(
                    hid[...].reshape(n_k * slots, units), rhs, FIRST, preferred_element_type=f32
                ).astype(bf16)

    def convolve():
        loads[10].wait()
        loads[9].wait()
        landed(early, "h", 0)
        earlier = jnp.where(seat.sp == 0, 0.0, early[tail_rows - 2:tail_rows, :])
        mixed = inner[...].astype(f32) * given[...].astype(f32)
        padded = jnp.concatenate([earlier, mixed], axis=0)
        t = taps[...].astype(f32)
        value = t[0:1] * padded[0:tokens] + t[1:2] * padded[1:tokens + 1]
        value = value + t[2:3] * mixed
        sum_ref[...] = value
        c_ref[0, 0] = (outer[...].astype(f32) * value).astype(bf16)
        for k in range(1, n_k):
            push(c_ref.at[0, 0], c_ref.at[k, 0], "cz", (k,), seat.over_z(k))
        push(c_ref.at[0, 0], c_ref.at[0, 1], "cx", (0,), seat.over_x())

    def spread():
        for k in range(1, n_k):
            landed(c_ref.at[k, 0], "cz", (k,))
            push(c_ref.at[k, 0], c_ref.at[k, 1], "cx", (k,), seat.over_x())

    items = [(kind, k) for k in order for kind in range(2)]
    last = len(items)
    near, far, deep = order[1], order[2], order[3]

    def chunk(item):
        kind, k = item
        s4(item)
        if kind == 0:
            pre(k)
        else:
            mid(k)
            post(k, 0, False)
            post(k, 1, False)
            post(k, 0, True)
            post(k, 1, True)

    for n in range(last + 3):
        if 2 <= n < last + 2:
            s2(items[n - 2])
        if 3 <= n < last + 3:
            s3(items[n - 3])
        if n < last:
            s1(items[n])
        if n == 3:
            for load in loads[6:9]:
                load.wait()
            convolve()
        if n == last - 1:
            spread()
        if n == last + 1:
            r2(0)
            r2(near)
        if n == last + 2:
            r3(0)
            r3(near)
            r2(far)
        if n >= 4:
            chunk(items[n - 4])
    r4(near)
    r3(far)
    chunk(items[-1])
    r4(0)
    r4(far)
    r2(deep)
    work(4)
    r3(deep)
    work(4)
    r4(deep)
    work(2)
    loads[11].wait()
    slice_width = g_ref.shape[3]
    share_rows = tokens // 2
    border = late.shape[0]
    ends = [(k, s) for k in order for s in range(2) if k or s]

    def gather():
        for k in range(1, n_k):
            landed(ret.at[k], "r4", (k,))
        moe = lax.dot_general(
            sel[...], ret[...].reshape(n_k * capacity, width), FIRST, preferred_element_type=f32
        )
        sg[:, my_cols] = total(block[1, :, my_cols], moe.astype(bf16))
        spot = sg.at[:, my_cols]
        push(spot, spot, "ag", 0, seat.over_y())
        push(spot, spot, "ag", 1, seat.other_core())

    def gather_y():
        spot = sg.at[:, y_cols]
        landed(spot, "ag", 0)
        push(spot, spot, "ag", 2, seat.other_core())

    def gather_rest():
        landed(sg.at[:, core_cols[0]], "ag", 1)
        landed(sg.at[:, core_cols[1]], "ag", 2)

    def piece(k, swap, core):
        d = seat.plane(k) * 2 + (ox if swap else seat.x)
        first = pl.ds(pl.multiple_of(core * share_rows, share_rows), share_rows)
        return sg.at[first, pl.ds(pl.multiple_of(d * slice_width, slice_width), slice_width)]

    def g_half(k, swap, core):
        first = pl.ds(pl.multiple_of(core * share_rows, share_rows), share_rows)
        return g_ref.at[k, swap, first, :]

    def g_send():
        for k, s in reversed(ends):
            push(piece(k, s, seat.c), g_half(k, s, seat.c), "g", (k, s), seat.over_z(k, s))

    def project():
        conv_grad = jnp.dot(sg[...], ow[...], preferred_element_type=f32)
        ext[0:tokens, :] = conv_grad * outer[...].astype(f32)
        push(ext.at[0:border, :], late, "h", 1, seat.next_tokens(-1))
        outer_grad[...] = (conv_grad * sum_ref[...]).astype(bf16)
        own = sg[:, pl.ds(pl.multiple_of(seat.sp * slice_width, slice_width), slice_width)]
        out_grad[...] = lax.dot_general(own, c_ref[0, 0], FIRST, preferred_element_type=f32)

    def finish_conv():
        landed(late, "h", 1)
        ext[tokens:tokens + border, :] = jnp.where(seat.sp == 2 * n_k - 1, 0.0, late[...])
        t = taps[...].astype(f32)
        mixed_grad = t[2:3] * ext[0:tokens, :]
        mixed_grad = mixed_grad + t[1:2] * ext[1:tokens + 1, :]
        mixed_grad = mixed_grad + t[0:1] * ext[2:tokens + 2, :]
        inner_grad[...] = (mixed_grad * given[...].astype(f32)).astype(bf16)
        input_grad[...] = (mixed_grad * inner[...].astype(f32)).astype(bf16)

    def g_wait(k, s):
        spot = g_half(k, s, seat.c)
        landed(spot, "g", (k, s))
        push(spot, spot, "gc", (k, s), seat.other_core())

    def g_add(k, s):
        landed(g_half(k, s, 1 - seat.c), "gc", (k, s))
        out_grad[...] += lax.dot_general(
            g_ref[k, s], c_ref[k, s], FIRST, preferred_element_type=f32
        )

    def drain():
        for copy in started:
            copy.wait_send()

    gather()
    work(2)
    gather_y()
    gather_rest()
    g_send()
    project()
    work(len(pieces))
    for k in range(n_k):
        landed(c_ref.at[k, 1], "cx", (k,))
    for k, s in ends[:4]:
        g_wait(k, s)
    finish_conv()
    for k, s in ends[4:]:
        g_wait(k, s)
    for k, s in ends:
        g_add(k, s)
    drain()


def write_kernel(count, *refs):
    sources, targets, done = refs[:count], refs[count:2 * count], refs[2 * count]
    copies = [pltpu.make_async_copy(sources[n], targets[n], done.at[n]) for n in range(count)]
    for copy in copies:
        copy.start()
    for copy in copies:
        copy.wait()


def in_vmem(count):
    return [pl.BlockSpec(memory_space=pltpu.VMEM)] * count


def in_hbm(count):
    return [pl.BlockSpec(memory_space=pltpu.HBM)] * count


def fused(cotangent, stream, routes, route_weights, gate, up, down, outer, inner, given, taps,
          out_weight, experts, capacity):
    tokens, model = stream.shape
    units = gate.shape[1]
    channels = outer.shape[1]
    width = model // 4
    slice_width = model // (2 * experts)
    border, tail_rows = min(8, tokens), min(16, tokens)
    cut = capacity // 2 // 16 * 16
    rest = capacity - cut
    bf16, f32 = jnp.bfloat16, jnp.float32
    n = experts
    slots = 2 * capacity
    gate_shape = jax.ShapeDtypeStruct((model, units), bf16)
    own = jax.ShapeDtypeStruct((tokens, channels), bf16)
    outs = (
        gate_shape, gate_shape, jax.ShapeDtypeStruct((units, model), bf16),
        jax.ShapeDtypeStruct((slice_width, channels), f32), own, own, own,
    )
    half = (n, 2, 2, capacity, width)
    scratch = [
        ((2, tokens), jnp.int32), ((2, tokens), f32), ((2, tokens, model), bf16),
        ((n * capacity, tokens), bf16), ((n, capacity, 1), f32),
        ((model, units), bf16), ((model, units), bf16), ((units, model), bf16),
        ((tokens, channels), bf16), ((tokens, channels), bf16), ((tokens, channels), bf16),
        ((3, channels), bf16), ((model, channels), bf16),
        ((2, n, capacity, width), bf16), ((n, 2, capacity, model), bf16),
        ((n, 2, capacity, model), bf16), ((slots, units), f32), ((slots, units), f32),
        ((n, slots, units), bf16), ((n, slots, 2 * units), bf16),
        (half, bf16), (half, bf16), (half, bf16), (half, bf16),
        ((n, 2, cut, width), bf16), ((n, 2, rest, width), bf16),
        ((n, 2, cut, width), bf16), ((n, 2, rest, width), bf16),
        ((n, cut, width), bf16), ((n, rest, width), bf16),
        ((n, capacity, width), bf16), ((n, capacity, width), bf16),
        ((tokens, model), bf16), ((n, 2, tokens, slice_width), bf16),
        ((n, 2, tokens, channels), bf16), ((tokens, channels), f32),
        ((tail_rows, channels), f32), ((tail_rows, channels), f32),
        ((tokens + border, channels), f32), ((border, channels), f32),
    ]
    sems = [pltpu.SemaphoreType.DMA((12,)), pltpu.SemaphoreType.DMA((1,))]
    for shape_of in SEMS.values():
        sems += [pltpu.SemaphoreType.DMA(shape_of(n))] * 2
    made = pl.pallas_call(
        functools.partial(fused_kernel, experts, capacity),
        out_shape=tuple(pltpu.VMEM(out.shape, out.dtype) for out in outs),
        in_specs=in_hbm(12),
        out_specs=tuple(in_vmem(7)),
        scratch_shapes=[pltpu.VMEM(*s) for s in scratch] + sems,
        compiler_params=pltpu.CompilerParams(
            collective_id=0, has_side_effects=True, vmem_limit_bytes=48 * 1024 * 1024
        ),
        name="fused",
    )(*[
        pltpu.with_memory_space_constraint(value, pltpu.HBM)
        for value in (
            routes.T, route_weights.T, stream, cotangent, gate, up, down, outer, inner, given,
            taps, out_weight,
        )
    ])
    written = pl.pallas_call(
        functools.partial(write_kernel, len(outs)),
        out_shape=outs,
        in_specs=in_vmem(len(outs)),
        out_specs=tuple(in_hbm(len(outs))),
        scratch_shapes=[pltpu.SemaphoreType.DMA((len(outs),))],
        compiler_params=pltpu.CompilerParams(vmem_limit_bytes=1024 * 1024),
        name="write",
    )(*made)
    return tuple(out[None] for out in written[:3]) + tuple(written[3:])


def per_device(
    cotangent,
    stream,
    routes,
    route_weights,
    gate_weight,
    up_weight,
    down_weight,
    outer_gate,
    inner_gate,
    conv_input,
    conv_taps,
    out_weight,
):
    groups = lax.axis_size("sp")
    tp_count = lax.axis_size("tp")
    experts = groups // 2
    tok_rows = stream.shape[0]
    model_width = stream.shape[1]
    capacity = 3 * tok_rows // experts
    slot_total = experts * capacity
    contract_first = (((0,), (0,)), ((), ()))
    contract_last = (((1,), (1,)), ((), ()))
    block_width = model_width // tp_count
    slots = groups * capacity
    even = experts & (experts - 1) == 0 and tp_count == 4
    if even and capacity % 32 == 0 and block_width % 128 == 0:
        return fused(
            cotangent, stream, routes, route_weights, gate_weight[0], up_weight[0],
            down_weight[0], outer_gate, inner_gate, conv_input, conv_taps, out_weight,
            experts, capacity,
        )
    taps = conv_taps.astype(jnp.float32)
    outer_f = outer_gate.astype(jnp.float32)
    inner_f = inner_gate.astype(jnp.float32)
    input_f = conv_input.astype(jnp.float32)
    mixed = inner_f * input_f
    flat_routes = routes.reshape(-1)
    choose = (flat_routes[:, None] == jnp.arange(experts, dtype=jnp.int32)[None, :]).astype(
        jnp.int32
    )
    before = jnp.cumsum(choose, axis=0) - choose
    slot_place = flat_routes * capacity + jnp.sum(before * choose, axis=1)
    slot_table = (jnp.arange(slot_total, dtype=jnp.int32)[:, None] == slot_place[None, :]).astype(
        jnp.float32
    )
    select = jnp.sum(slot_table.reshape(slot_total, tok_rows, 2), axis=2).astype(jnp.bfloat16)
    slot_weight = jnp.sum(slot_table * route_weights.reshape(-1)[None, :], axis=1)
    offset = lax.axis_index("tp") * block_width
    rows_part = lax.dynamic_slice_in_dim(stream, offset, block_width, 1)
    cot_part = lax.dynamic_slice_in_dim(cotangent, offset, block_width, 1)
    sent_rows = jnp.dot(select, rows_part, preferred_element_type=jnp.float32).astype(jnp.bfloat16)
    sent_cot = (
        jnp.dot(select, cot_part, preferred_element_type=jnp.float32) * slot_weight[:, None]
    ).astype(jnp.bfloat16)
    sent_rows = jnp.repeat(sent_rows.reshape(experts, capacity, -1), 2, axis=0)
    sent_cot = jnp.repeat(sent_cot.reshape(experts, capacity, -1), 2, axis=0)
    recv_rows, recv_cot = (
        lax.all_to_all(sent_rows, "sp", split_axis=0, concat_axis=0, tiled=True),
        lax.all_to_all(sent_cot, "sp", split_axis=0, concat_axis=0, tiled=True),
    )
    recv_rows, recv_cot = (
        lax.all_gather(recv_rows, "tp", axis=2, tiled=True),
        lax.all_gather(recv_cot, "tp", axis=2, tiled=True),
    )
    routed_rows = recv_rows.reshape(slots, model_width)
    routed_cot = recv_cot.reshape(slots, model_width)
    earlier = from_behind(mixed[-2:], "sp", 1)
    gate_local = gate_weight[0]
    up_local = up_weight[0]
    down_local = down_weight[0]
    gate_pre = jnp.dot(routed_rows, gate_local, preferred_element_type=jnp.float32)
    up_pre = jnp.dot(routed_rows, up_local, preferred_element_type=jnp.float32)
    hidden_grad = lax.dot_general(
        routed_cot, down_local, contract_last, preferred_element_type=jnp.float32
    )
    sigma = jax.nn.sigmoid(gate_pre)
    silu_gate = gate_pre * sigma
    hidden = (silu_gate * up_pre).astype(jnp.bfloat16)
    up_delta = (hidden_grad * silu_gate).astype(jnp.bfloat16)
    gate_delta = (hidden_grad * up_pre * sigma * (1.0 + gate_pre * (1.0 - sigma))).astype(
        jnp.bfloat16
    )
    row_partial = lax.dot_general(
        gate_delta, gate_local, contract_last, preferred_element_type=jnp.float32
    )
    row_partial = row_partial + lax.dot_general(
        up_delta, up_local, contract_last, preferred_element_type=jnp.float32
    )
    padded = jnp.concatenate([earlier, mixed], axis=0)
    conv_sum = taps[0] * padded[:-2] + taps[1] * padded[1:-1] + taps[2] * padded[2:]
    conv_out = (outer_f * conv_sum).astype(jnp.bfloat16)
    gate_grad = lax.dot_general(
        routed_rows, gate_delta, contract_first, preferred_element_type=jnp.float32
    ).astype(jnp.bfloat16)[None]
    up_grad = lax.dot_general(
        routed_rows, up_delta, contract_first, preferred_element_type=jnp.float32
    ).astype(jnp.bfloat16)[None]
    down_grad = lax.dot_general(
        hidden, routed_cot, contract_first, preferred_element_type=jnp.float32
    ).astype(jnp.bfloat16)[None]
    half_sums = lax.psum_scatter(
        row_partial.astype(jnp.bfloat16), "tp", scatter_dimension=1, tiled=True
    ).astype(jnp.float32)
    block_width = half_sums.shape[1]
    half_grad = half_sums.reshape(groups, capacity, block_width).astype(jnp.bfloat16)
    returned = lax.all_to_all(half_grad, "sp", split_axis=0, concat_axis=0, tiled=True)
    returned = returned.reshape(experts, 2, capacity, block_width)
    select_three = select.reshape(experts, capacity, tok_rows)
    moe_part = jnp.einsum(
        "ecr,emcd->rd", select_three, returned, preferred_element_type=jnp.float32
    ).astype(jnp.bfloat16)
    moe_grad = lax.all_gather(moe_part, "tp", axis=1, tiled=True)
    stream_grad = (cotangent.astype(jnp.float32) + moe_grad.astype(jnp.float32)).astype(
        jnp.bfloat16
    )
    out_grad = lax.psum_scatter(
        lax.dot_general(
            stream_grad, conv_out, contract_first, preferred_element_type=jnp.float32
        ).astype(jnp.bfloat16),
        "sp",
        scatter_dimension=0,
        tiled=True,
    ).astype(jnp.float32)
    conv_grad = jnp.dot(stream_grad, out_weight, preferred_element_type=jnp.float32)
    outer_grad = (conv_grad * conv_sum).astype(jnp.bfloat16)
    scaled = conv_grad * outer_f
    later = from_behind(scaled[:2], "sp", -1)
    extended = jnp.concatenate([scaled, later], axis=0)
    mixed_grad = taps[2] * extended[:-2] + taps[1] * extended[1:-1] + taps[0] * extended[2:]
    inner_grad = (mixed_grad * input_f).astype(jnp.bfloat16)
    input_grad = (mixed_grad * inner_f).astype(jnp.bfloat16)
    return (gate_grad, up_grad, down_grad, out_grad, outer_grad, inner_grad, input_grad)


def solution(mesh):
    placed = (
        P("sp", None),
        P("sp", None),
        P("sp", None),
        P("sp", None),
        P("sp", None, "tp"),
        P("sp", None, "tp"),
        P("sp", "tp", None),
        P("sp", "tp"),
        P("sp", "tp"),
        P("sp", "tp"),
        P(None, "tp"),
        P(None, "tp"),
    )
    return jax.shard_map(
        per_device,
        mesh=mesh,
        in_specs=placed,
        out_specs=(
            P("sp", None, "tp"),
            P("sp", None, "tp"),
            P("sp", "tp", None),
            P("sp", "tp"),
            P("sp", "tp"),
            P("sp", "tp"),
            P("sp", "tp"),
        ),
        check_vma=False,
    )
```

time: 115 us -> 86.8 us (0.75)
  the two profiles are of different devices: /device:TPU:5 before, /device:TPU:0 now
where the time goes in v1:
time: 86.8 us; the launch traced here: 86.6 us
  Pallas kernels  85.8 us (99%)
    pallas_call x1, Pallas kernels, fused(): pl.pallas_call(functools.partial(fused_kernel, experts, capacity), out_sh...  83 us
    pallas_call x1, Pallas kernels, fused(): pl.pallas_call(functools.partial(write_kernel, len(outs)), out_shape=outs...  2.82 us

profile of v1, /device:TPU:0, one launch (start us, length us, event | category | flops | bytes accessed | tf_op | source)
XLA Modules:
  0.0 86.6 jit_solution(9603626285545655686)
XLA Ops:
  0.6 83.0 %fused.1 = (bf16[2048,512]{1,0:T(8,128)(2,1)S(1)}, bf16[2048,512]{1,0:T(8,128)(2,1)S(1)}, bf16[512,2048]{1,0:T(8,128)(2,1)S(1)}, f32[256,256]{1,0:T(8,128)S(1)},...) custom-call(s32[2,128]{1,0:T(2,128)} %bitcast.11, f32[2,128]{1,0:T(2,128)} %bitcast.12, ...), custom_call_target="tpu_custom_call" | custom-call | tf_op jit(solution)/shard_map/fused/pallas_call | solution.py:560
  83.7 2.8 %write.1 = (bf16[2048,512]{1,0:T(8,128)(2,1)}, bf16[2048,512]{1,0:T(8,128)(2,1)}, bf16[512,2048]{1,0:T(8,128)(2,1)}, f32[256,256]{1,0:T(8,128)}, bf16[128,256]{1...) custom-call(bf16[2048,512]{1,0:T(8,128)(2,1)S(1)} %get-tuple-element.21.refs_0_, ...), custom_call_target="tpu_custom_call" | custom-call | tf_op jit(solution)/shard_map/write/pallas_call | solution.py:577

commit v2 on v1

--- a/solution.py
+++ b/solution.py
@@ -43,6 +43,13 @@
             weight *= 2
         return number
 
+    def between(self, plane):
+        number, weight = 0, 1
+        while weight < self.experts:
+            number = number + weight * lax.rem(self.z // weight + plane // weight, 2)
+            weight *= 2
+        return number
+
     def over_z(self, k, swap=0):
         return (self.plane(k) * 2 + (1 - self.x if swap else self.x), self.tp)
 
@@ -61,10 +68,11 @@
 
 
 SEMS = {
-    "z": lambda n: (2, n), "x": lambda n: (2, n), "y": lambda n: (2, n), "d": lambda n: (2, n, 2),
-    "c": lambda n: (2, n, 4), "r1": lambda n: (n, 2), "r2": lambda n: (n, 2),
-    "r3": lambda n: (n, 2), "r4": lambda n: (n,), "ag": lambda n: (3,), "g": lambda n: (n, 2),
-    "gc": lambda n: (n, 2), "cz": lambda n: (n,), "cx": lambda n: (n,), "h": lambda n: (2,),
+    "z": lambda n: (2, n), "x": lambda n: (2, n), "y": lambda n: (2, n), "d": lambda n: (2, n),
+    "c0": lambda n: (2,), "c": lambda n: (2, n), "r1": lambda n: (n,), "r2": lambda n: (n, 2),
+    "r3": lambda n: (n, 2), "r4": lambda n: (1,), "ag": lambda n: (3,), "g": lambda n: (n, 2),
+    "gc": lambda n: (1,), "cz": lambda n: (1,), "cx": lambda n: (1,), "h0": lambda n: (1,),
+    "h1": lambda n: (1,),
 }
 
 FIRST = (((0,), (0,)), ((), ()))
@@ -86,10 +94,9 @@
      send, rows, cots, gp_ref, up_ref, hid, delta, part, mine_part, a_ref, acc, b1a, b1b, acc2a,
      acc2b, b2a, b2b, fin, ret, sg, g_ref, c_ref, sum_ref, tail_ref, early, ext,
      late) = take(40)
-    load_sem, keep_sem = take(2)
-    sem = {}
-    for name in SEMS:
-        sem[name] = take(2)
+    load_sem, sent_sem = take(2)
+    names = list(SEMS)
+    sem = dict(zip(names, take(len(names))))
     seat = Seat(experts)
     n_k = experts
     tokens, model = block.shape[1:]
@@ -99,7 +106,6 @@
     places = (rows, cots)
     slots = 2 * capacity
     f32, bf16 = jnp.float32, jnp.bfloat16
-    started = []
 
     barrier = pltpu.get_barrier_semaphore()
     peers = [seat.over_z(k, s) for k in range(n_k) for s in range(2) if k or s]
@@ -117,14 +123,10 @@
         pl.semaphore_signal(barrier, inc=1, device_id=peer, device_id_type=pl.DeviceIdType.MESH)
 
     def push(src, dst, name, at, device):
-        sent, got = sem[name]
-        copy = remote(src, dst, sent.at[at], got.at[at], device)
-        copy.start()
-        started.append(copy)
+        remote(src, dst, sent_sem.at[names.index(name)], sem[name].at[at], device).start()
 
     def landed(spot, name, at):
-        sent, got = sem[name]
-        remote(spot, spot, sent.at[at], got.at[at], seat.other_core()).wait_recv()
+        remote(spot, spot, sent_sem.at[0], sem[name].at[at], seat.other_core()).wait_recv()
 
     def cols(tp):
         return pl.ds(pl.multiple_of(tp * width, width), width)
@@ -147,7 +149,7 @@
         loads[5].wait()
         tail_ref[...] = inner[edge, :].astype(f32) * given[edge, :].astype(f32)
         pl.semaphore_wait(barrier, len(peers))
-        push(tail_ref, early, "h", 0, seat.next_tokens(1))
+        push(tail_ref, early, "h0", 0, seat.next_tokens(1))
 
     loads[0].wait()
     loads[1].wait()
@@ -181,20 +183,19 @@
             got = got * slot_weight[k]
         return got.astype(bf16)
 
-    order = list(range(n_k))
+    order = [0] + [k for k in range(1, n_k) if k != 2] + [2]
 
     def fill(k, kind):
-        if k == order[1]:
-            loads[2 + kind].wait()
         send[kind, k] = pick(kind, k, my_cols)
-        if k == order[1] and kind == 0:
-            send_halo()
+
+    def launch(k, kind):
         push(send.at[kind, k], places[kind].at[k, seat.x, :, my_cols], "z", (kind, k),
              seat.over_z(k))
 
-    for k in order[1:]:
-        for kind in range(2):
-            fill(k, kind)
+    def fill_own(kind):
+        for tp in range(model // width):
+            span = slice(tp * width, (tp + 1) * width)
+            places[kind][0, seat.x, :, span] = pick(kind, 0, span)
 
     def spot_of(item, x, span):
         kind, k = item
@@ -206,12 +207,13 @@
 
     ox = 1 - seat.x
 
+    def to_core(spot, item):
+        kind, k = item
+        push(spot, spot, "c" if k else "c0", item if k else kind, seat.other_core())
+
     def s1(item):
         kind, k = item
         if k == 0:
-            for tp in range(model // width):
-                span = slice(tp * width, (tp + 1) * width)
-                places[kind][0, seat.x, :, span] = pick(kind, 0, span)
             spot = spot_of(item, seat.x, my_cols)
             push(spot, spot, "x", item, seat.over_x())
         else:
@@ -219,7 +221,7 @@
             landed(spot, "z", item)
             push(spot, spot, "x", item, seat.over_x())
             push(spot, spot, "y", item, seat.over_y())
-            push(spot, spot, "c", item + (0,), seat.other_core())
+            push(spot, spot, "c", item, seat.other_core())
 
     def s2(item):
         kind, k = item
@@ -229,14 +231,14 @@
             push(spot, spot, "y", item, seat.over_y())
         else:
             part_spot = half_of(item, ox, my_cols, 0)
-            push(part_spot, part_spot, "d", item + (0,), seat.over_y())
-        push(spot, spot, "c", item + (1,), seat.other_core())
+            push(part_spot, part_spot, "d", item, seat.over_y())
+        to_core(spot, item)
         if k:
             spot = spot_of(item, seat.x, y_cols)
             landed(spot, "y", item)
             part_spot = half_of(item, seat.x, y_cols, 1)
-            push(part_spot, part_spot, "d", item + (1,), seat.over_x())
-            push(spot, spot, "c", item + (2,), seat.other_core())
+            push(part_spot, part_spot, "d", item, seat.over_x())
+            push(spot, spot, "c", item, seat.other_core())
 
     def s3(item):
         kind, k = item
@@ -244,16 +246,15 @@
         if k == 0:
             landed(spot, "y", item)
         else:
-            landed(half_of(item, ox, y_cols, 0), "d", item + (0,))
-            landed(half_of(item, ox, y_cols, 1), "d", item + (1,))
-        push(spot, spot, "c", item + (3,), seat.other_core())
+            landed(spot, "d", item)
+        to_core(spot, item)
 
     def s4(item):
         kind, k = item
-        for j in range(4):
-            if k == 0 and j % 2 == 0:
-                continue
-            landed(spot_of(item, ox if j % 2 else seat.x, core_cols[j // 2]), "c", item + (j,))
+        if k == 0:
+            landed(rows.at[0, :, :, 0:width], "c0", kind)
+        else:
+            landed(rows.at[k, :, :, 0:2 * width], "c", item)
 
     tile = 256 if units % 256 == 0 else units
 
@@ -288,11 +289,11 @@
             )
             out[k, y, :, :, at:at + tile] = value.astype(bf16).reshape(2, capacity, tile)
         if not mine:
-            push(part.at[k, y], a_ref.at[k, y], "r1", (k, y), seat.other_core())
+            push(part.at[k, y], a_ref.at[k, y], "r1", k, seat.other_core())
 
     def r2(k):
+        landed(a_ref.at[k], "r1", k)
         for y in range(2):
-            landed(a_ref.at[k, y], "r1", (k, y))
             acc[k, y] = total(mine_part[k, y], a_ref[k, y])
         push(acc.at[k, :, ox, pl.ds(0, cut), :], b1a.at[k], "r2", (k, 0), seat.over_x())
         push(acc.at[k, 1 - seat.y, :, pl.ds(cut, capacity - cut), :], b1b.at[k], "r2", (k, 1),
@@ -315,7 +316,7 @@
         out[0:cut, :] = total(acc2a[k, seat.y], b2a[k])
         out[cut:capacity, :] = total(acc2b[k, seat.x], b2b[k])
         if k:
-            push(fin.at[k], ret.at[k], "r4", (k,), seat.over_z(k))
+            push(fin.at[k], ret.at[k], "r4", 0, seat.over_z(k))
 
     step = 256 if model % 256 == 0 else model
     pieces = [(0, at) for at in range(0, model, step)] + [(1, at) for at in range(0, model, 2 * step)]
@@ -337,10 +338,13 @@
                     hid[...].reshape(n_k * slots, units), rhs, FIRST, preferred_element_type=f32
                 ).astype(bf16)
 
+    share_rows = tokens // 2
+    slice_width = g_ref.shape[4]
+
     def convolve():
         loads[10].wait()
         loads[9].wait()
-        landed(early, "h", 0)
+        landed(early, "h0", 0)
         earlier = jnp.where(seat.sp == 0, 0.0, early[tail_rows - 2:tail_rows, :])
         mixed = inner[...].astype(f32) * given[...].astype(f32)
         padded = jnp.concatenate([earlier, mixed], axis=0)
@@ -348,74 +352,113 @@
         value = t[0:1] * padded[0:tokens] + t[1:2] * padded[1:tokens + 1]
         value = value + t[2:3] * mixed
         sum_ref[...] = value
-        c_ref[0, 0] = (outer[...].astype(f32) * value).astype(bf16)
+        value = (outer[...].astype(f32) * value).astype(bf16)
+        for j in range(2):
+            c_ref[j, 0, 0] = value[j * share_rows:(j + 1) * share_rows]
+
+    def spread_z():
         for k in range(1, n_k):
-            push(c_ref.at[0, 0], c_ref.at[k, 0], "cz", (k,), seat.over_z(k))
-        push(c_ref.at[0, 0], c_ref.at[0, 1], "cx", (0,), seat.over_x())
-
-    def spread():
-        for k in range(1, n_k):
-            landed(c_ref.at[k, 0], "cz", (k,))
-            push(c_ref.at[k, 0], c_ref.at[k, 1], "cx", (k,), seat.over_x())
+            push(c_ref.at[:, 0, 0], c_ref.at[:, k, 0], "cz", 0, seat.over_z(k))
+
+    def spread_x():
+        landed(c_ref.at[:, 1:n_k, 0], "cz", 0)
+        for k in range(n_k):
+            push(c_ref.at[:, k, 0], c_ref.at[:, k, 1], "cx", 0, seat.over_x())
 
     items = [(kind, k) for k in order for kind in range(2)]
     last = len(items)
     near, far, deep = order[1], order[2], order[3]
 
-    def chunk(item):
-        kind, k = item
-        s4(item)
-        if kind == 0:
-            pre(k)
-        else:
-            mid(k)
-            post(k, 0, False)
-            post(k, 1, False)
-            post(k, 0, True)
-            post(k, 1, True)
-
-    for n in range(last + 3):
-        if 2 <= n < last + 2:
-            s2(items[n - 2])
-        if 3 <= n < last + 3:
-            s3(items[n - 3])
-        if n < last:
-            s1(items[n])
-        if n == 3:
-            for load in loads[6:9]:
-                load.wait()
-            convolve()
-        if n == last - 1:
-            spread()
-        if n == last + 1:
-            r2(0)
-            r2(near)
-        if n == last + 2:
-            r3(0)
-            r3(near)
-            r2(far)
-        if n >= 4:
-            chunk(items[n - 4])
+    def experts_of(k):
+        mid(k)
+        post(k, 0, False)
+        post(k, 1, False)
+        post(k, 0, True)
+        post(k, 1, True)
+
+    loads[2].wait()
+    fill(near, 0)
+    fill_own(0)
+    send_halo()
+    s1(items[0])
+    launch(near, 0)
+    loads[3].wait()
+    fill(near, 1)
+    launch(near, 1)
+    fill_own(1)
+    s1(items[1])
+    for k in order[2:]:
+        for kind in range(2):
+            fill(k, kind)
+            launch(k, kind)
+    s2(items[0])
+    s1(items[2])
+    s2(items[1])
+    s3(items[0])
+    s1(items[3])
+    for load in loads[6:9]:
+        load.wait()
+    convolve()
+    s2(items[2])
+    s3(items[1])
+    s1(items[4])
+    s4(items[0])
+    pre(0)
+    s2(items[3])
+    s3(items[2])
+    s1(items[5])
+    s4(items[1])
+    experts_of(0)
+    s2(items[4])
+    s3(items[3])
+    s1(items[6])
+    s4(items[2])
+    pre(near)
+    s2(items[5])
+    s3(items[4])
+    s1(items[7])
+    spread_z()
+    s4(items[3])
+    experts_of(near)
+    s2(items[6])
+    s3(items[5])
+    s4(items[4])
+    pre(far)
+    s2(items[7])
+    r2(0)
+    r2(near)
+    s4(items[5])
+    experts_of(far)
+    s3(items[6])
+    s3(items[7])
+    r2(far)
+    s4(items[6])
+    pre(deep)
+    r3(0)
+    r3(near)
+    s4(items[7])
+    mid(deep)
+    post(deep, 0, False)
+    post(deep, 1, False)
+    r3(far)
+    post(deep, 0, True)
+    post(deep, 1, True)
     r4(near)
-    r3(far)
-    chunk(items[-1])
+    r2(deep)
     r4(0)
     r4(far)
-    r2(deep)
-    work(4)
+    work(6)
     r3(deep)
+    spread_x()
     work(4)
     r4(deep)
     work(2)
     loads[11].wait()
-    slice_width = g_ref.shape[3]
-    share_rows = tokens // 2
     border = late.shape[0]
     ends = [(k, s) for k in order for s in range(2) if k or s]
 
     def gather():
-        for k in range(1, n_k):
-            landed(ret.at[k], "r4", (k,))
+        landed(ret.at[1:n_k], "r4", 0)
         moe = lax.dot_general(
             sel[...], ret[...].reshape(n_k * capacity, width), FIRST, preferred_element_type=f32
         )
@@ -424,38 +467,53 @@
         push(spot, spot, "ag", 0, seat.over_y())
         push(spot, spot, "ag", 1, seat.other_core())
 
+    def flip(bits):
+        number, weight = 0, 1
+        while weight < n_k:
+            number = number + weight * lax.rem(bits // weight + seat.tp // weight, 2)
+            weight *= 2
+        return number
+
+    def g_half(k, swap, core):
+        return g_ref.at[core, k, swap]
+
+    mine_half = pl.ds(pl.multiple_of(seat.c * share_rows, share_rows), share_rows)
+
+    def g_send(j):
+        plane = flip(j)
+        k = seat.between(plane)
+        for s in range(2):
+            d = plane * 2 + (ox if s else seat.x)
+            src = sg.at[mine_half, pl.ds(pl.multiple_of(d * slice_width, slice_width), slice_width)]
+            if s:
+                push(src, g_half(k, s, seat.c), "g", (k, s), (d, seat.tp))
+            else:
+                @pl.when(k > 0)
+                def _():
+                    push(src, g_half(k, s, seat.c), "g", (k, s), (d, seat.tp))
+
+    def gather_core():
+        landed(sg.at[:, core_cols[0]], "ag", 1)
+
     def gather_y():
         spot = sg.at[:, y_cols]
         landed(spot, "ag", 0)
         push(spot, spot, "ag", 2, seat.other_core())
 
     def gather_rest():
-        landed(sg.at[:, core_cols[0]], "ag", 1)
         landed(sg.at[:, core_cols[1]], "ag", 2)
-
-    def piece(k, swap, core):
-        d = seat.plane(k) * 2 + (ox if swap else seat.x)
-        first = pl.ds(pl.multiple_of(core * share_rows, share_rows), share_rows)
-        return sg.at[first, pl.ds(pl.multiple_of(d * slice_width, slice_width), slice_width)]
-
-    def g_half(k, swap, core):
-        first = pl.ds(pl.multiple_of(core * share_rows, share_rows), share_rows)
-        return g_ref.at[k, swap, first, :]
-
-    def g_send():
-        for k, s in reversed(ends):
-            push(piece(k, s, seat.c), g_half(k, s, seat.c), "g", (k, s), seat.over_z(k, s))
 
     def project():
         conv_grad = jnp.dot(sg[...], ow[...], preferred_element_type=f32)
         ext[0:tokens, :] = conv_grad * outer[...].astype(f32)
-        push(ext.at[0:border, :], late, "h", 1, seat.next_tokens(-1))
+        push(ext.at[0:border, :], late, "h1", 0, seat.next_tokens(-1))
         outer_grad[...] = (conv_grad * sum_ref[...]).astype(bf16)
-        own = sg[:, pl.ds(pl.multiple_of(seat.sp * slice_width, slice_width), slice_width)]
-        out_grad[...] = lax.dot_general(own, c_ref[0, 0], FIRST, preferred_element_type=f32)
+        own = pl.ds(pl.multiple_of(seat.sp * slice_width, slice_width), slice_width)
+        for j in range(2):
+            g_ref[j, 0, 0] = sg[j * share_rows:(j + 1) * share_rows, own]
 
     def finish_conv():
-        landed(late, "h", 1)
+        landed(late, "h1", 0)
         ext[tokens:tokens + border, :] = jnp.where(seat.sp == 2 * n_k - 1, 0.0, late[...])
         t = taps[...].astype(f32)
         mixed_grad = t[2:3] * ext[0:tokens, :]
@@ -467,34 +525,54 @@
     def g_wait(k, s):
         spot = g_half(k, s, seat.c)
         landed(spot, "g", (k, s))
-        push(spot, spot, "gc", (k, s), seat.other_core())
-
-    def g_add(k, s):
-        landed(g_half(k, s, 1 - seat.c), "gc", (k, s))
-        out_grad[...] += lax.dot_general(
-            g_ref[k, s], c_ref[k, s], FIRST, preferred_element_type=f32
+        push(spot, spot, "gc", 0, seat.other_core())
+
+    def g_add(core):
+        rows_of = 2 * n_k * share_rows
+        return lax.dot_general(
+            g_ref[core].reshape(rows_of, slice_width), c_ref[core].reshape(rows_of, -1), FIRST,
+            preferred_element_type=f32,
         )
 
+    def g_own():
+        landed(c_ref.at[:, :, 1], "cx", 0)
+        out_grad[...] = g_add(seat.c)
+
+    def g_other():
+        landed(sg.at[0:share_rows, 0:len(ends) * slice_width], "gc", 0)
+        out_grad[...] += g_add(1 - seat.c)
+
     def drain():
-        for copy in started:
-            copy.wait_send()
+        pieces_sent = sg.at[0:share_rows, 0:len(ends) * slice_width]
+        spans = {
+            "z": send.at[:, 1:n_k], "x": rows.at[:, :, :, 0:width], "y": rows.at[:, :, :, 0:width],
+            "d": send.at[:, 1:n_k], "c0": rows.at[0:2, :, :, 0:width], "c": rows.at[0:n_k - 1],
+            "r1": part, "r2": part.at[:, 0], "r3": part.at[:, 0, 0], "r4": part.at[0:n_k - 1, 0, 0],
+            "ag": sg.at[:, 0:3 * width], "g": pieces_sent, "gc": pieces_sent,
+            "cz": c_ref.at[:, 1:n_k, 0], "cx": c_ref.at[:, :, 0], "h0": tail_ref,
+            "h1": ext.at[0:border, :],
+        }
+        for n, name in enumerate(names):
+            span = spans[name]
+            remote(span, span, sent_sem.at[n], load_sem.at[0], seat.other_core()).wait_send()
 
     gather()
-    work(2)
+    g_send(0)
+    gather_core()
+    g_send(1)
+    work(len(pieces))
     gather_y()
+    g_send(2)
     gather_rest()
-    g_send()
+    g_send(3)
     project()
-    work(len(pieces))
-    for k in range(n_k):
-        landed(c_ref.at[k, 1], "cx", (k,))
     for k, s in ends[:4]:
         g_wait(k, s)
     finish_conv()
     for k, s in ends[4:]:
         g_wait(k, s)
-    for k, s in ends:
-        g_add(k, s)
+    g_own()
+    g_other()
     drain()
 
 
@@ -549,14 +627,13 @@
         ((n, 2, cut, width), bf16), ((n, 2, rest, width), bf16),
         ((n, cut, width), bf16), ((n, rest, width), bf16),
         ((n, capacity, width), bf16), ((n, capacity, width), bf16),
-        ((tokens, model), bf16), ((n, 2, tokens, slice_width), bf16),
-        ((n, 2, tokens, channels), bf16), ((tokens, channels), f32),
+        ((tokens, model), bf16), ((2, n, 2, tokens // 2, slice_width), bf16),
+        ((2, n, 2, tokens // 2, channels), bf16), ((tokens, channels), f32),
         ((tail_rows, channels), f32), ((tail_rows, channels), f32),
         ((tokens + border, channels), f32), ((border, channels), f32),
     ]
-    sems = [pltpu.SemaphoreType.DMA((12,)), pltpu.SemaphoreType.DMA((1,))]
-    for shape_of in SEMS.values():
-        sems += [pltpu.SemaphoreType.DMA(shape_of(n))] * 2
+    sems = [pltpu.SemaphoreType.DMA((12,)), pltpu.SemaphoreType.DMA((len(SEMS),))]
+    sems += [pltpu.SemaphoreType.DMA(shape_of(n)) for shape_of in SEMS.values()]
     made = pl.pallas_call(
         functools.partial(fused_kernel, experts, capacity),
         out_shape=tuple(pltpu.VMEM(out.shape, out.dtype) for out in outs),
@@ -611,7 +688,7 @@
     contract_last = (((1,), (1,)), ((), ()))
     block_width = model_width // tp_count
     slots = groups * capacity
-    even = experts & (experts - 1) == 0 and tp_count == 4
+    even = experts == tp_count == 4
     if even and capacity % 32 == 0 and block_width % 128 == 0:
         return fused(
             cotangent, stream, routes, route_weights, gate_weight[0], up_weight[0],

time: 86.8 us -> 72 us (0.83)
  the two profiles are of different devices: /device:TPU:0 before, /device:TPU:5 now
where the time goes in v2:
time: 72 us; the launch traced here: 71.9 us
  Pallas kernels  71.1 us (99%)
  between operations  0.81 us (1%)
    pallas_call x1, Pallas kernels, fused(): pl.pallas_call(functools.partial(fused_kernel, experts, capacity), out_sh...  68.2 us
    pallas_call x1, Pallas kernels, fused(): pl.pallas_call(functools.partial(write_kernel, len(outs)), out_shape=outs...  2.82 us

profile of v2, /device:TPU:5, one launch (start us, length us, event | category | flops | bytes accessed | tf_op | source)
XLA Modules:
  0.0 71.9 jit_solution(3704278001739628263)
XLA Ops:
  0.6 68.2 %fused.1 = (bf16[2048,512]{1,0:T(8,128)(2,1)S(1)}, bf16[2048,512]{1,0:T(8,128)(2,1)S(1)}, bf16[512,2048]{1,0:T(8,128)(2,1)S(1)}, f32[256,256]{1,0:T(8,128)S(1)},...) custom-call(s32[2,128]{1,0:T(2,128)} %bitcast.11, f32[2,128]{1,0:T(2,128)} %bitcast.12, ...), custom_call_target="tpu_custom_call" | custom-call | tf_op jit(solution)/shard_map/fused/pallas_call | solution.py:637
  68.9 2.8 %write.1 = (bf16[2048,512]{1,0:T(8,128)(2,1)}, bf16[2048,512]{1,0:T(8,128)(2,1)}, bf16[512,2048]{1,0:T(8,128)(2,1)}, f32[256,256]{1,0:T(8,128)}, bf16[128,256]{1...) custom-call(bf16[2048,512]{1,0:T(8,128)(2,1)S(1)} %get-tuple-element.21.refs_0_, ...), custom_call_target="tpu_custom_call" | custom-call | tf_op jit(solution)/shard_map/write/pallas_call | solution.py:654

commit v3 on v2

--- a/solution.py
+++ b/solution.py
@@ -149,7 +149,10 @@
         loads[5].wait()
         tail_ref[...] = inner[edge, :].astype(f32) * given[edge, :].astype(f32)
         pl.semaphore_wait(barrier, len(peers))
-        push(tail_ref, early, "h0", 0, seat.next_tokens(1))
+
+        @pl.when(seat.sp < 2 * n_k - 1)
+        def _():
+            push(tail_ref, early, "h0", 0, seat.next_tokens(1))
 
     loads[0].wait()
     loads[1].wait()
@@ -183,14 +186,15 @@
             got = got * slot_weight[k]
         return got.astype(bf16)
 
-    order = [0] + [k for k in range(1, n_k) if k != 2] + [2]
+    order = list(range(n_k))
 
     def fill(k, kind):
         send[kind, k] = pick(kind, k, my_cols)
 
     def launch(k, kind):
+        plane = seat.between(k)
         push(send.at[kind, k], places[kind].at[k, seat.x, :, my_cols], "z", (kind, k),
-             seat.over_z(k))
+             (plane * 2 + seat.x, seat.tp))
 
     def fill_own(kind):
         for tp in range(model // width):
@@ -203,7 +207,9 @@
 
     def half_of(item, x, span, j):
         kind, k = item
-        return places[kind].at[k, x, pl.ds(cut, capacity - cut) if j else pl.ds(0, cut), span]
+        edge_at = capacity // 3 // 16 * 16
+        part_rows = pl.ds(edge_at, capacity - edge_at) if j else pl.ds(0, edge_at)
+        return places[kind].at[k, x, part_rows, span]
 
     ox = 1 - seat.x
 
@@ -223,7 +229,7 @@
             push(spot, spot, "y", item, seat.over_y())
             push(spot, spot, "c", item, seat.other_core())
 
-    def s2(item):
+    def s2x(item):
         kind, k = item
         spot = spot_of(item, ox, my_cols)
         landed(spot, "x", item)
@@ -233,12 +239,13 @@
             part_spot = half_of(item, ox, my_cols, 0)
             push(part_spot, part_spot, "d", item, seat.over_y())
         to_core(spot, item)
-        if k:
-            spot = spot_of(item, seat.x, y_cols)
-            landed(spot, "y", item)
-            part_spot = half_of(item, seat.x, y_cols, 1)
-            push(part_spot, part_spot, "d", item, seat.over_x())
-            push(spot, spot, "c", item, seat.other_core())
+
+    def s2y(item):
+        spot = spot_of(item, seat.x, y_cols)
+        landed(spot, "y", item)
+        part_spot = half_of(item, seat.x, y_cols, 1)
+        push(part_spot, part_spot, "d", item, seat.over_x())
+        to_core(spot, item)
 
     def s3(item):
         kind, k = item
@@ -261,15 +268,15 @@
     def pre(k):
         lhs = rows[k].reshape(slots, model)
         for at in range(0, units, tile):
-            gp_ref[:, at:at + tile] = jnp.dot(lhs, gate[:, at:at + tile], preferred_element_type=f32)
-            up_ref[:, at:at + tile] = jnp.dot(lhs, up[:, at:at + tile], preferred_element_type=f32)
+            gp_ref[int(k == 1), :, at:at + tile] = jnp.dot(lhs, gate[:, at:at + tile], preferred_element_type=f32)
+            up_ref[int(k == 1), :, at:at + tile] = jnp.dot(lhs, up[:, at:at + tile], preferred_element_type=f32)
 
     def mid(k):
         lhs = cots[k].reshape(slots, model)
         for at in range(0, units, tile):
             span = slice(at, at + tile)
             grad = lax.dot_general(lhs, down[span, :], LAST, preferred_element_type=f32)
-            gate_pre, up_pre = gp_ref[:, span], up_ref[:, span]
+            gate_pre, up_pre = gp_ref[int(k == 1), :, span], up_ref[int(k == 1), :, span]
             sigma = jax.nn.sigmoid(gate_pre)
             silu = gate_pre * sigma
             hid[k, :, span] = (silu * up_pre).astype(bf16)
@@ -344,8 +351,15 @@
     def convolve():
         loads[10].wait()
         loads[9].wait()
-        landed(early, "h0", 0)
-        earlier = jnp.where(seat.sp == 0, 0.0, early[tail_rows - 2:tail_rows, :])
+        @pl.when(seat.sp > 0)
+        def _():
+            landed(early, "h0", 0)
+
+        @pl.when(seat.sp == 0)
+        def _():
+            early[...] = jnp.zeros_like(early)
+
+        earlier = early[tail_rows - 2:tail_rows, :]
         mixed = inner[...].astype(f32) * given[...].astype(f32)
         padded = jnp.concatenate([earlier, mixed], axis=0)
         t = taps[...].astype(f32)
@@ -365,95 +379,17 @@
         for k in range(n_k):
             push(c_ref.at[:, k, 0], c_ref.at[:, k, 1], "cx", 0, seat.over_x())
 
-    items = [(kind, k) for k in order for kind in range(2)]
-    last = len(items)
-    near, far, deep = order[1], order[2], order[3]
-
-    def experts_of(k):
-        mid(k)
+    near, far, cross = 1, 2, 3
+    items = [(kind, k) for k in (0, near, cross, far) for kind in range(2)]
+
+    def away(k):
         post(k, 0, False)
         post(k, 1, False)
+
+    def keep(k):
         post(k, 0, True)
         post(k, 1, True)
 
-    loads[2].wait()
-    fill(near, 0)
-    fill_own(0)
-    send_halo()
-    s1(items[0])
-    launch(near, 0)
-    loads[3].wait()
-    fill(near, 1)
-    launch(near, 1)
-    fill_own(1)
-    s1(items[1])
-    for k in order[2:]:
-        for kind in range(2):
-            fill(k, kind)
-            launch(k, kind)
-    s2(items[0])
-    s1(items[2])
-    s2(items[1])
-    s3(items[0])
-    s1(items[3])
-    for load in loads[6:9]:
-        load.wait()
-    convolve()
-    s2(items[2])
-    s3(items[1])
-    s1(items[4])
-    s4(items[0])
-    pre(0)
-    s2(items[3])
-    s3(items[2])
-    s1(items[5])
-    s4(items[1])
-    experts_of(0)
-    s2(items[4])
-    s3(items[3])
-    s1(items[6])
-    s4(items[2])
-    pre(near)
-    s2(items[5])
-    s3(items[4])
-    s1(items[7])
-    spread_z()
-    s4(items[3])
-    experts_of(near)
-    s2(items[6])
-    s3(items[5])
-    s4(items[4])
-    pre(far)
-    s2(items[7])
-    r2(0)
-    r2(near)
-    s4(items[5])
-    experts_of(far)
-    s3(items[6])
-    s3(items[7])
-    r2(far)
-    s4(items[6])
-    pre(deep)
-    r3(0)
-    r3(near)
-    s4(items[7])
-    mid(deep)
-    post(deep, 0, False)
-    post(deep, 1, False)
-    r3(far)
-    post(deep, 0, True)
-    post(deep, 1, True)
-    r4(near)
-    r2(deep)
-    r4(0)
-    r4(far)
-    work(6)
-    r3(deep)
-    spread_x()
-    work(4)
-    r4(deep)
-    work(2)
-    loads[11].wait()
     border = late.shape[0]
     ends = [(k, s) for k in order for s in range(2) if k or s]
 
@@ -506,15 +442,26 @@
     def project():
         conv_grad = jnp.dot(sg[...], ow[...], preferred_element_type=f32)
         ext[0:tokens, :] = conv_grad * outer[...].astype(f32)
-        push(ext.at[0:border, :], late, "h1", 0, seat.next_tokens(-1))
+
+        @pl.when(seat.sp > 0)
+        def _():
+            push(ext.at[0:border, :], late, "h1", 0, seat.next_tokens(-1))
+
         outer_grad[...] = (conv_grad * sum_ref[...]).astype(bf16)
         own = pl.ds(pl.multiple_of(seat.sp * slice_width, slice_width), slice_width)
         for j in range(2):
             g_ref[j, 0, 0] = sg[j * share_rows:(j + 1) * share_rows, own]
 
     def finish_conv():
-        landed(late, "h1", 0)
-        ext[tokens:tokens + border, :] = jnp.where(seat.sp == 2 * n_k - 1, 0.0, late[...])
+        @pl.when(seat.sp < 2 * n_k - 1)
+        def _():
+            landed(late, "h1", 0)
+            ext[tokens:tokens + border, :] = late[...]
+
+        @pl.when(seat.sp == 2 * n_k - 1)
+        def _():
+            ext[tokens:tokens + border, :] = jnp.zeros_like(late)
+
         t = taps[...].astype(f32)
         mixed_grad = t[2:3] * ext[0:tokens, :]
         mixed_grad = mixed_grad + t[1:2] * ext[1:tokens + 1, :]
@@ -552,12 +499,140 @@
             "cz": c_ref.at[:, 1:n_k, 0], "cx": c_ref.at[:, :, 0], "h0": tail_ref,
             "h1": ext.at[0:border, :],
         }
-        for n, name in enumerate(names):
-            span = spans[name]
-            remote(span, span, sent_sem.at[n], load_sem.at[0], seat.other_core()).wait_send()
-
+
+        def wait_sent(name):
+            span, at = spans[name], names.index(name)
+            remote(span, span, sent_sem.at[at], load_sem.at[0], seat.other_core()).wait_send()
+
+        for name in names:
+            if name == "h0":
+                pl.when(seat.sp < 2 * n_k - 1)(functools.partial(wait_sent, name))
+            elif name == "h1":
+                pl.when(seat.sp > 0)(functools.partial(wait_sent, name))
+            else:
+                wait_sent(name)
+
+    inner_plane = (seat.z + seat.z // 2) % 2
+
+    def first_wave(kind):
+        launch(near + inner_plane * (cross - near), kind)
+
+        @pl.when(inner_plane == 1)
+        def _():
+            launch(near, kind)
+
+    def second_wave():
+        for kind in range(2):
+            launch(cross - inner_plane * (cross - far), kind)
+
+    def third_wave():
+        @pl.when(inner_plane == 0)
+        def _():
+            for kind in range(2):
+                launch(far, kind)
+
+    loads[2].wait()
+    fill(near, 0)
+    fill(cross, 0)
+    fill_own(0)
+    send_halo()
+    s1(items[0])
+    first_wave(0)
+    loads[3].wait()
+    fill(near, 1)
+    fill(cross, 1)
+    first_wave(1)
+    fill_own(1)
+    s1(items[1])
+    fill(far, 0)
+    fill(far, 1)
+    s1(items[2])
+    s2x(items[0])
+    second_wave()
+    s1(items[3])
+    s2y(items[2])
+    third_wave()
+    s2x(items[1])
+    s2x(items[2])
+    s2x(items[3])
+    s1(items[4])
+    s2y(items[3])
+    s3(items[0])
+    s1(items[5])
+    s3(items[1])
+    s4(items[0])
+    s3(items[2])
+    s2x(items[4])
+    for load in loads[6:9]:
+        load.wait()
+    pre(0)
+    s1(items[6])
+    s2y(items[4])
+    s4(items[2])
+    s4(items[1])
+    convolve()
+    s3(items[3])
+    mid(0)
+    s2x(items[5])
+    post(0, 1, True)
+    post(0, 0, True)
+    s4(items[3])
+    s2y(items[5])
+    post(0, 1, False)
+    pre(near)
+    s1(items[7])
+    spread_z()
+    s3(items[4])
+    mid(near)
+    post(0, 0, False)
+    s2y(items[6])
+    post(near, 1, True)
+    s2x(items[6])
+    s3(items[5])
+    s4(items[4])
+    pre(cross)
+    post(near, 0, False)
+    r2(0)
+    post(near, 0, True)
+    s2x(items[7])
+    s2y(items[7])
+    post(near, 1, False)
+    s3(items[6])
+    s4(items[5])
+    mid(cross)
+    post(cross, 0, True)
+    post(cross, 1, False)
+    r2(near)
+    s4(items[6])
+    post(cross, 0, False)
+    pre(far)
+    s3(items[7])
+    post(cross, 1, True)
+    r2(cross)
+    s4(items[7])
+    r3(0)
+    mid(far)
+    r3(near)
+    post(far, 1, False)
+    post(far, 0, False)
+    post(far, 0, True)
+    post(far, 1, True)
+    r3(cross)
+    r2(far)
+    r4(0)
+    r4(near)
+    work(2)
+    r4(cross)
+    work(1)
+    r3(far)
+    spread_x()
+    work(3)
+    r4(far)
+    work(3)
     gather()
     g_send(0)
+    work(3)
+    loads[11].wait()
     gather_core()
     g_send(1)
     work(len(pieces))
@@ -566,11 +641,9 @@
     gather_rest()
     g_send(3)
     project()
-    for k, s in ends[:4]:
+    for k, s in ends:
         g_wait(k, s)
     finish_conv()
-    for k, s in ends[4:]:
-        g_wait(k, s)
     g_own()
     g_other()
     drain()
@@ -578,11 +651,14 @@
 
 def write_kernel(count, *refs):
     sources, targets, done = refs[:count], refs[count:2 * count], refs[2 * count]
-    copies = [pltpu.make_async_copy(sources[n], targets[n], done.at[n]) for n in range(count)]
-    for copy in copies:
-        copy.start()
-    for copy in copies:
-        copy.wait()
+    for n in range(count):
+        rows = sources[n].shape[0]
+        step = rows // 8 if rows % 128 == 0 and rows > 256 else rows
+        for at in range(0, rows, step):
+            span = pl.ds(at, step)
+            pltpu.make_async_copy(sources[n].at[span], targets[n].at[span], done.at[n]).start()
+    for n in range(count):
+        pltpu.make_async_copy(sources[n], targets[n], done.at[n]).wait()
 
 
 def in_vmem(count):
@@ -620,7 +696,7 @@
         ((tokens, channels), bf16), ((tokens, channels), bf16), ((tokens, channels), bf16),
         ((3, channels), bf16), ((model, channels), bf16),
         ((2, n, capacity, width), bf16), ((n, 2, capacity, model), bf16),
-        ((n, 2, capacity, model), bf16), ((slots, units), f32), ((slots, units), f32),
+        ((n, 2, capacity, model), bf16), ((2, slots, units), f32), ((2, slots, units), f32),
         ((n, slots, units), bf16), ((n, slots, 2 * units), bf16),
         (half, bf16), (half, bf16), (half, bf16), (half, bf16),
         ((n, 2, cut, width), bf16), ((n, 2, rest, width), bf16),

time: 72 us -> 71.4 us (level)
  no operation moved by 1% of the time
where the time goes in v3:
time: 71.4 us; the launch traced here: 71.2 us
  Pallas kernels  70.4 us (99%)
  between operations  0.81 us (1%)
    pallas_call x1, Pallas kernels, fused(): pl.pallas_call(functools.partial(fused_kernel, experts, capacity), out_sh...  67.6 us
    pallas_call x1, Pallas kernels, fused(): pl.pallas_call(functools.partial(write_kernel, len(outs)), out_shape=outs...  2.82 us

profile of v3, /device:TPU:5, one launch (start us, length us, event | category | flops | bytes accessed | tf_op | source)
XLA Modules:
  0.0 71.2 jit_solution(2020386971012009510)
XLA Ops:
  0.6 67.6 %fused.1 = (bf16[2048,512]{1,0:T(8,128)(2,1)S(1)}, bf16[2048,512]{1,0:T(8,128)(2,1)S(1)}, bf16[512,2048]{1,0:T(8,128)(2,1)S(1)}, f32[256,256]{1,0:T(8,128)S(1)},...) custom-call(s32[2,128]{1,0:T(2,128)} %bitcast.11, f32[2,128]{1,0:T(2,128)} %bitcast.12, ...), custom_call_target="tpu_custom_call" | custom-call | tf_op jit(solution)/shard_map/fused/pallas_call | solution.py:713
  68.3 2.8 %write.1 = (bf16[2048,512]{1,0:T(8,128)(2,1)}, bf16[2048,512]{1,0:T(8,128)(2,1)}, bf16[512,2048]{1,0:T(8,128)(2,1)}, f32[256,256]{1,0:T(8,128)}, bf16[128,256]{1...) custom-call(bf16[2048,512]{1,0:T(8,128)(2,1)S(1)} %get-tuple-element.21.refs_0_, ...), custom_call_target="tpu_custom_call" | custom-call | tf_op jit(solution)/shard_map/write/pallas_call | solution.py:730

commit v4 on v3

--- a/solution.py
+++ b/solution.py
@@ -69,7 +69,7 @@
 
 SEMS = {
     "z": lambda n: (2, n), "x": lambda n: (2, n), "y": lambda n: (2, n), "d": lambda n: (2, n),
-    "c0": lambda n: (2,), "c": lambda n: (2, n), "r1": lambda n: (n,), "r2": lambda n: (n, 2),
+    "c0": lambda n: (2,), "c": lambda n: (2, n), "r1": lambda n: (n,), "r2": lambda n: (n, 4),
     "r3": lambda n: (n, 2), "r4": lambda n: (1,), "ag": lambda n: (3,), "g": lambda n: (n, 2),
     "gc": lambda n: (1,), "cz": lambda n: (1,), "cx": lambda n: (1,), "h0": lambda n: (1,),
     "h1": lambda n: (1,),
@@ -302,28 +302,30 @@
         landed(a_ref.at[k], "r1", k)
         for y in range(2):
             acc[k, y] = total(mine_part[k, y], a_ref[k, y])
-        push(acc.at[k, :, ox, pl.ds(0, cut), :], b1a.at[k], "r2", (k, 0), seat.over_x())
-        push(acc.at[k, 1 - seat.y, :, pl.ds(cut, capacity - cut), :], b1b.at[k], "r2", (k, 1),
-             seat.over_y())
+        for j, (y, x) in enumerate(((1 - seat.y, ox), (seat.y, seat.x))):
+            push(acc.at[k, y, ox, pl.ds(0, cut), :], b1a.at[k, y], "r2", (k, 2 * j), seat.over_x())
+            push(acc.at[k, 1 - seat.y, x, pl.ds(cut, capacity - cut), :], b1b.at[k, x], "r2",
+                 (k, 2 * j + 1), seat.over_y())
 
     def r3(k):
-        landed(b1a.at[k], "r2", (k, 0))
-        for y in range(2):
+        for j, (y, x) in enumerate(((1 - seat.y, ox), (seat.y, seat.x))):
+            landed(b1a.at[k, y], "r2", (k, 2 * j))
             acc2a[k, y] = total(acc[k, y, seat.x, 0:cut, :], b1a[k, y])
-        push(acc2a.at[k, 1 - seat.y], b2a.at[k], "r3", (k, 0), seat.over_y())
-        landed(b1b.at[k], "r2", (k, 1))
-        for x in range(2):
+            if j == 0:
+                push(acc2a.at[k, y], b2a.at[k], "r3", (k, 0), seat.over_y())
+            landed(b1b.at[k, x], "r2", (k, 2 * j + 1))
             acc2b[k, x] = total(acc[k, seat.y, x, cut:capacity, :], b1b[k, x])
-        push(acc2b.at[k, ox], b2b.at[k], "r3", (k, 1), seat.over_x())
+            if j == 0:
+                push(acc2b.at[k, x], b2b.at[k], "r3", (k, 1), seat.over_x())
 
     def r4(k):
-        landed(b2a.at[k], "r3", (k, 0))
-        landed(b2b.at[k], "r3", (k, 1))
         out = fin.at[k] if k else ret.at[0]
-        out[0:cut, :] = total(acc2a[k, seat.y], b2a[k])
-        out[cut:capacity, :] = total(acc2b[k, seat.x], b2b[k])
-        if k:
-            push(fin.at[k], ret.at[k], "r4", 0, seat.over_z(k))
+        for j, (mine, theirs) in enumerate(((acc2a, b2a), (acc2b, b2b))):
+            landed(theirs.at[k], "r3", (k, j))
+            span = pl.ds(cut, capacity - cut) if j else pl.ds(0, cut)
+            out[span, :] = total(mine[k, seat.x if j else seat.y], theirs[k])
+            if k:
+                push(fin.at[k, span], ret.at[k, span], "r4", 0, seat.over_z(k))
 
     step = 256 if model % 256 == 0 else model
     pieces = [(0, at) for at in range(0, model, step)] + [(1, at) for at in range(0, model, 2 * step)]

time: 71.4 us -> 70.7 us (level)
  no operation moved by 1% of the time
where the time goes in v4:
time: 70.7 us; the launch traced here: 70.6 us
  Pallas kernels  69.8 us (99%)
  between operations  0.81 us (1%)
    pallas_call x1, Pallas kernels, fused(): pl.pallas_call(functools.partial(fused_kernel, experts, capacity), out_sh...  66.9 us
    pallas_call x1, Pallas kernels, fused(): pl.pallas_call(functools.partial(write_kernel, len(outs)), out_shape=outs...  2.82 us

profile of v4, /device:TPU:5, one launch (start us, length us, event | category | flops | bytes accessed | tf_op | source)
XLA Modules:
  0.0 70.6 jit_solution(16832259984899724106)
XLA Ops:
  0.6 66.9 %fused.1 = (bf16[2048,512]{1,0:T(8,128)(2,1)S(1)}, bf16[2048,512]{1,0:T(8,128)(2,1)S(1)}, bf16[512,2048]{1,0:T(8,128)(2,1)S(1)}, f32[256,256]{1,0:T(8,128)S(1)},...) custom-call(s32[2,128]{1,0:T(2,128)} %bitcast.11, f32[2,128]{1,0:T(2,128)} %bitcast.12, ...), custom_call_target="tpu_custom_call" | custom-call | tf_op jit(solution)/shard_map/fused/pallas_call | solution.py:715
  67.6 2.8 %write.1 = (bf16[2048,512]{1,0:T(8,128)(2,1)}, bf16[2048,512]{1,0:T(8,128)(2,1)}, bf16[512,2048]{1,0:T(8,128)(2,1)}, f32[256,256]{1,0:T(8,128)}, bf16[128,256]{1...) custom-call(bf16[2048,512]{1,0:T(8,128)(2,1)S(1)} %get-tuple-element.21.refs_0_, ...), custom_call_target="tpu_custom_call" | custom-call | tf_op jit(solution)/shard_map/write/pallas_call | solution.py:732
